TPU v7x, 256 devices: a whole 4x4x8 slice. The times are simulated.
256 devices in a mesh: sp: 64 (over z, y, core), tp: 4 (over x).
Axes of the slice: x: 4, y: 4, z: 8, core: 2. Of those that a mesh axis runs over, the one named last changes fastest.
Arguments:
- resid: bfloat16 [16384, 2048], P(('sp', 'tp')), may hold values from -6 to 6
- queries: bfloat16 [16384, 1024], P('sp', 'tp'), may hold values from -6 to 6
- keys: bfloat16 [16384, 256], P('sp', 'tp'), may hold values from -6 to 6
- values: bfloat16 [16384, 256], P('sp', 'tp'), may hold values from -6 to 6
- docs: int32 [16384], P('sp'), may hold values from 0 to 31, never falling along the last dimension, each value on 1 to 1024 neighbouring positions
- q_gain: float32 [64], replicated, may hold values from 0.1 to 1.9
- key_norm_gain: float32 [64], replicated, may hold values from 0.1 to 1.9
- sink: float32 [16], P('tp'), may hold values from 4 to 8
- out_gain: float32 [1024], replicated, may hold values from 0.1 to 1.9
- w_out: bfloat16 [1024, 2048], replicated, may hold values from -0.1875 to 0.1875
- norm_gain: float32 [2048], replicated, may hold values from 0.1 to 1.9
- routes: int32 [16384, 4], P('sp'), may hold values from 0 to 63, all different within a row; in each aligned block of 64 rows (0 to 63, 64 to 127, ...) at most 8 rows name the same one
- route_weights: float32 [16384, 4], P(('sp', 'tp')), may hold values from 0.1 to 1
- w_gate: bfloat16 [64, 2048, 2048], P('sp', None, 'tp'), may hold values from -0.375 to 0.375
- w_up: bfloat16 [64, 2048, 2048], P('sp', None, 'tp'), may hold values from -0.375 to 0.375
- w_down: bfloat16 [64, 2048, 2048], P('sp', 'tp'), may hold values from -0.015625 to 0.015625
Outputs:
- layer_out: bfloat16 [16384, 2048], P(('sp', 'tp'))
Inputs may be any that keep to these rules, and one draw needn't show every extreme that they name: `routes`: in each aligned block of 64 tokens no expert is named more than 8 times, and some expert is named exactly that often; the 4 experts of a token differ. `docs`: document numbers never fall along the sequence, and each document has 1 to 1024 positions.
All inputs are finite; a program needn't handle non-finite values.
Results may differ from a plain program's by a relative error of at most 0.015.
Values may be sent and summed in bfloat16 or wider, within the bound.
A program may use at most 128 MiB of HBM per device.

v0:
```python
import jax
import jax.numpy as jnp
from jax import lax
from jax.sharding import PartitionSpec as P

WINDOW = 128


rope_base = 10000.0
norm_eps = 1e-06
swiglu_limit = 7.0
swiglu_alpha = 1.702


def extended(x, sides, width):
    for axis, dim in sides:
        peers, length = (lax.axis_size(axis), x.shape[dim])
        up = [(i, (i + 1) % peers) for i in range(peers - 1)]
        down = [(j, i) for i, j in up]
        last = lax.slice_in_dim(x, length - width, length, axis=dim)
        leading = lax.slice_in_dim(x, 0, width, axis=dim)
        before = lax.ppermute(last, axis, up)
        after = lax.ppermute(leading, axis, down)
        x = jnp.concatenate([before, x, after], axis=dim)
    return x


def in_order(parts, dim):
    dims = list(parts.shape[1:])
    dims[dim] *= parts.shape[0]
    return jnp.moveaxis(parts, 0, dim).reshape(dims)


def piecewise(x, axis, dim, work, out_dim):
    width = x.shape[dim]
    pieces = jnp.split(x, 2, axis=dim) if width % 2 == 0 else [x]
    leading = jnp.arange(lax.axis_size(axis)) * width
    parts = [lax.all_gather(section, axis) for section in pieces]
    made = [jax.vmap(work)(b, leading + k * (width // len(pieces))) for k, b in enumerate(parts)]
    return in_order(jnp.concatenate(made, axis=out_dim + 1), out_dim)


def row_normalize(values, gain_vec):
    floats = values.astype(jnp.float32)
    scale_inv = lax.rsqrt(jnp.mean(floats * floats, axis=-1, keepdims=True) + norm_eps)
    return floats * scale_inv * gain_vec


def apply_rotary_heads(heads, token_positions):
    half_size = heads.shape[-1] // 2
    freqs = rope_base ** (-jnp.arange(half_size, dtype=jnp.float32) / half_size)
    angles = token_positions[:, None] * freqs[None, :]
    cosine = jnp.cos(angles)[:, None, :]
    sine = jnp.sin(angles)[:, None, :]
    first_half = heads[..., :half_size]
    second_half = heads[..., half_size:]
    return jnp.concatenate(
        [first_half * cosine - second_half * sine, first_half * sine + second_half * cosine],
        axis=-1,
    )


def expert_act(gate_pre, up_pre):
    gate_cut = jnp.minimum(gate_pre, swiglu_limit)
    up_cut = jnp.clip(up_pre, -swiglu_limit, swiglu_limit)
    return (up_cut + 1.0) * gate_cut * jax.nn.sigmoid(swiglu_alpha * gate_cut)


def slot_tables(route_block, expert_count, capacity):
    pair_total = route_block.shape[1]
    expert_ids = jnp.arange(expert_count, dtype=jnp.int32)
    onehot = (route_block[:, :, None] == expert_ids[None, None, :]).astype(jnp.int32)
    before = jnp.cumsum(onehot, axis=1) - onehot
    rank = jnp.sum(before * onehot, axis=-1)
    pair_slot = route_block * capacity + rank
    slot_ids = jnp.arange(expert_count * capacity, dtype=jnp.int32)
    match = pair_slot[:, :, None] == slot_ids[None, None, :]
    pair_ids = jnp.arange(pair_total, dtype=jnp.int32)
    slot_pair = jnp.sum(jnp.where(match, pair_ids[None, :, None], 0), axis=1)
    filled = jnp.any(match, axis=1)
    return (pair_slot, slot_pair, filled)


def expert_partial(arrived_rows, w_gate, w_up, w_down):
    lead_shape = arrived_rows.shape
    local_experts = w_gate.shape[0]
    grouped = arrived_rows.reshape(-1, local_experts, lead_shape[2] // local_experts, lead_shape[3])
    gate_pre = jnp.einsum("recd,edf->recf", grouped, w_gate, preferred_element_type=jnp.float32)
    up_pre = jnp.einsum("recd,edf->recf", grouped, w_up, preferred_element_type=jnp.float32)
    hidden = expert_act(gate_pre, up_pre).astype(jnp.bfloat16)
    partial_value = jnp.einsum("recf,efd->recd", hidden, w_down, preferred_element_type=jnp.float32)
    return (
        lax.optimization_barrier(partial_value.astype(jnp.bfloat16))
        .astype(jnp.float32)
        .reshape(lead_shape)
    )


def per_device(
    resid,
    queries,
    keys,
    values,
    docs,
    q_gain,
    key_norm_gain,
    sink,
    out_gain,
    w_out,
    norm_gain,
    routes,
    route_weights,
    w_gate,
    w_up,
    w_down,
):
    sp_size = lax.axis_size("sp")
    tp_size = lax.axis_size("tp")
    sp_index = lax.axis_index("sp")
    tp_index = lax.axis_index("tp")
    tok_rows = queries.shape[0]
    head_size = q_gain.shape[0]
    query_heads = sink.shape[0]
    kv_heads = keys.shape[1] // head_size
    query_group_width = query_heads // kv_heads
    token_positions = (sp_index * tok_rows + jnp.arange(tok_rows, dtype=jnp.int32)).astype(
        jnp.float32
    )
    q_rot = apply_rotary_heads(
        row_normalize(queries.reshape(tok_rows, query_heads, head_size), q_gain), token_positions
    ).astype(jnp.bfloat16)
    key_rotated = apply_rotary_heads(
        row_normalize(keys.reshape(tok_rows, kv_heads, head_size), key_norm_gain), token_positions
    ).astype(jnp.bfloat16)
    key_value = jnp.concatenate(
        [key_rotated.reshape(tok_rows, kv_heads * head_size), values], axis=1
    )
    doc_mark = (docs + 1).astype(jnp.bfloat16)
    kv_span, doc_span = (
        extended(key_value, (("sp", 0),), WINDOW),
        extended(doc_mark, (("sp", 0),), WINDOW),
    )
    span_rows = tok_rows + 2 * WINDOW
    k_span = kv_span[:, : kv_heads * head_size].reshape(span_rows, kv_heads, head_size)
    v_span = kv_span[:, kv_heads * head_size :].reshape(span_rows, kv_heads, head_size)
    scores = jnp.einsum(
        "qhgd,khd->hgqk",
        q_rot.reshape(tok_rows, kv_heads, query_group_width, head_size),
        k_span,
        preferred_element_type=jnp.float32,
    ) * head_size ** (-0.5)
    offsets = jnp.arange(tok_rows, dtype=jnp.int32)[:, None] - (
        jnp.arange(span_rows, dtype=jnp.int32)[None, :] - WINDOW
    )
    allowed = (jnp.abs(offsets) <= WINDOW) & (doc_mark[:, None] == doc_span[None, :])
    raw_weights = jnp.where(allowed[None, None], jnp.exp(scores), jnp.zeros((), jnp.float32))
    sink_exponent = jnp.exp(sink).reshape(kv_heads, query_group_width)
    total = jnp.sum(raw_weights, axis=-1) + sink_exponent[:, :, None]
    probs = (raw_weights / total[..., None]).astype(jnp.bfloat16)
    att = jnp.einsum("hgqk,khd->qhgd", probs, v_span, preferred_element_type=jnp.float32)
    att = att.astype(jnp.bfloat16).reshape(tok_rows, query_heads * head_size)
    by_token = lax.all_to_all(att, "tp", split_axis=0, concat_axis=1, tiled=True)
    att_normed = row_normalize(by_token, out_gain).astype(jnp.bfloat16)
    middle = (
        resid.astype(jnp.float32) + jnp.dot(att_normed, w_out, preferred_element_type=jnp.float32)
    ).astype(jnp.bfloat16)
    moe_in = row_normalize(middle, norm_gain).astype(jnp.bfloat16)
    quarter = tok_rows // tp_size
    top_count = routes.shape[1]
    local_experts = w_gate.shape[0]
    expert_count = sp_size * local_experts
    capacity = 3 * quarter * top_count // (2 * expert_count) + 2
    model_width = moe_in.shape[1]
    empty = jnp.zeros((), jnp.bfloat16)
    own_routes = lax.dynamic_slice_in_dim(routes, tp_index * quarter, quarter, 0)
    pair_slot, slot_pair, filled = slot_tables(
        own_routes.reshape(1, quarter * top_count), expert_count, capacity
    )
    outgoing = jnp.where(filled[:, :, None], moe_in[slot_pair // top_count], empty)
    outgoing = outgoing.reshape(1, sp_size, local_experts * capacity, model_width)
    arrived = lax.all_to_all(outgoing, "sp", split_axis=1, concat_axis=1, tiled=True)

    def term_piece(block_piece, first_row):
        return expert_partial(block_piece, w_gate, w_up, w_down)

    terms = piecewise(arrived, "tp", 0, term_piece, 0)
    summed = lax.psum_scatter(terms.astype(jnp.bfloat16), "tp", scatter_dimension=0, tiled=True)
    own_slot = pair_slot[0]
    returned = lax.all_to_all(summed, "sp", split_axis=1, concat_axis=1, tiled=True)
    picked = returned.reshape(-1, model_width)[own_slot].reshape(quarter, top_count, model_width)
    routed = jnp.sum(picked.astype(jnp.float32) * route_weights[:, :, None], axis=1)
    return (middle.astype(jnp.float32) + routed).astype(jnp.bfloat16)


def solution(mesh):
    return jax.shard_map(
        per_device,
        mesh=mesh,
        in_specs=(
            P(("sp", "tp"), None),
            P("sp", "tp"),
            P("sp", "tp"),
            P("sp", "tp"),
            P("sp"),
            P(),
            P(),
            P("tp"),
            P(),
            P(),
            P(),
            P("sp", None),
            P(("sp", "tp"), None),
            P("sp", None, "tp"),
            P("sp", None, "tp"),
            P("sp", "tp", None),
        ),
        out_specs=P(("sp", "tp"), None),
        check_vma=False,
    )
```

profile of v0, /device:TPU:8, one launch (start us, length us, event | category | flops | bytes accessed | tf_op | source)
XLA Modules:
  0.0 384.8 jit_solution(17801195262215288850)
XLA Ops:
  6.6 0.9 fusion.23
  7.5 0.8 fusion.25
  8.3 0.2 fusion.36
  8.6 0.8 pad_maximum_fusion.1
  9.3 1.9 collective-permute-start
  11.3 3.6 collective-permute-start.1
  14.9 0.7 add_convert_fusion.2
  15.6 1.9 collective-permute-start.2
  17.5 3.6 collective-permute-start.3
  21.2 0.2 multiply_cosine_fusion
  21.4 0.8 broadcast_multiply_fusion
  22.1 0.1 copy.47
  22.2 0.1 reshape.668
  22.3 0.1 compare_convert_fusion
  22.4 0.6 reduce-window.6
  23.0 0.2 slice_reduce_fusion
  23.2 0.1 copy.49
  23.3 0.1 copy.50
  23.4 0.1 broadcast.469
  23.5 0.1 fusion.26
  23.7 0.1 select_reduce_fusion
  23.8 0.2 fusion.14
  24.0 1.0 copy.43
  25.1 0.1 multiply_multiply_fusion
  25.3 0.1 broadcast_in_dim.32
  25.4 0.0 collective-permute-done.2
  25.4 0.0 collective-permute-done.3
  25.4 0.2 fusion.15
  25.6 0.0 collective-permute-done
  25.6 0.0 collective-permute-done.1
  25.7 0.7 fusion.11
  26.4 0.1 broadcast_add_fusion
  26.4 0.6 fusion.12
  27.1 0.0 copy-start.1
  27.1 0.0 copy-start.4
  27.1 0.2 reshape.715
  27.2 0.8 copy.60
  28.1 4.3 %all-to-all-start = ((bf16[4,64,256]{2,1,0:T(8,128)(2,1)}), bf16[4,64,256]{2,1,0:T(8,128)(2,1)S(1)}, u32[]{:S(2)}, u32[]{:S(2)}) async-start(bf16[4,64,256]{2,1,0:T(8,128)(2,1)} %copy.60), calls=%async_computation | async-start | bytes 262144 | tf_op jit(solution)/shard_map/all_to_all | solution.py:162
  32.4 6.0 %all-to-all-done = bf16[4,64,256]{2,1,0:T(8,128)(2,1)S(1)} async-done(((bf16[4,64,256]{2,1,0:T(8,128)(2,1)}), bf16[4,64,256]{2,1,0:T(8,128)(2,1)S(1)}, u32[]{:S(2)}, u32[]{:S(2)}) %all-to-all-start) | async-done | bytes 131104 | tf_op jit(solution)/shard_map/all_to_all | solution.py:162
  38.4 0.1 fusion.16
  38.5 0.0 copy-done.4
  38.5 0.0 copy-start.3
  38.6 3.2 multiply_reduce_fusion.1
  41.8 0.0 copy-done.3
  41.8 0.1 multiply_convert_fusion.1
  41.9 3.3 gather_fusion
  45.3 1.8 bitcast_select_fusion
  47.1 67.3 %all_to_all.23 = bf16[1,64,8,2048]{3,2,0,1:T(8,128)(2,1)} all-to-all(bf16[1,64,8,2048]{3,2,0,1:T(8,128)(2,1)S(1)} %bitcast_select_fusion), channel_id=1, replica_groups=mesh['sp'=64,'tp'=4] {'sp'}, dimensions={1} | all-to-all | bytes 4194304 | tf_op jit(solution)/shard_map/all_to_all | solution.py:181
  114.3 0.0 all-gather.3.cloned.1.call-update
  114.3 0.2 reduce-scatter.2.cloned.1.call-start
  114.6 79.9 %all-gather.3.cloned.1.call-done = bf16[4,64,8,2048]{3,2,1,0:T(8,128)(2,1)} async-done(((bf16[1,64,8,2048]{3,2,1,0:T(8,128)(2,1)}), bf16[4,64,8,2048]{3,2,1,0:T(8,128)(2,1)}) %all-gather.3.cloned.1.call-update) | async-done | bytes 8388624 | tf_op jit(solution)/shard_map/all_gather | solution.py:38
  194.5 10.4 %fusion.5 = f32[4,64,8,512]{3,2,1,0:T(8,128)} fusion(bf16[4,64,8,2048]{3,2,1,0:T(8,128)(2,1)} %all-gather.3.cloned.1.call-done, bf16[1,2048,512]{2,1,0:T(8,128)(2,1)} %param.30), kind=kOutput, calls=%fused_computation.9 | convolution fusion | flops 4294967296 | bytes 14680064 | tf_op jit(solution)/shard_map/vmap(recd,edf->recf)/dot_general | solution.py:89
  204.8 14.9 %convert_bitcast_fusion = bf16[4,64,1,8,2048]{4,3,1,0,2:T(8,128)(2,1)} fusion(f32[4,64,8,512]{3,2,1,0:T(8,128)} %fusion.5, bf16[4,64,8,2048]{3,2,1,0:T(8,128)(2,1)} %all-gather.3.cloned.1.call-done, bf16[1,512,2048]{2,1,0:T(8,128)(2,1)S(1)} %copy-done, bf16[1,2048,512]{2,1,0:T(8,128)(2,1)} %param.29), kind=kOutput, calls=%fused_computation.2 | convolution fusion | flops 8604614656 | bytes 25165824 | tf_op jit(solution)/shard_map/vmap(recf,efd->recd)/dot_general | solution.py:91
  219.8 0.0 reduce-scatter.2.cloned.1.call-update
  219.8 84.2 %reduce-scatter.2.cloned.1.call-done = bf16[1,64,8,2048]{3,2,1,0:T(8,128)(2,1)} async-done(((bf16[4,64,8,2048]{3,2,1,0:T(8,128)(2,1)}), bf16[1,64,8,2048]{3,2,1,0:T(8,128)(2,1)}) %reduce-scatter.2.cloned.1.call-update) | async-done | bytes 2097168 | tf_op jit(solution)/shard_map/reduce_scatter | solution.py:187
  304.0 10.9 %all-to-all-start.2 = ((bf16[1,64,8,2048]{3,2,0,1:T(8,128)(2,1)}), bf16[1,64,8,2048]{3,2,0,1:T(8,128)(2,1)}, u32[]{:S(2)}, u32[]{:S(2)}) async-start(bf16[1,64,8,2048]{3,2,0,1:T(8,128)(2,1)} %bitcast.102), calls=%async_computation.3 | async-start | bytes 4194304 | tf_op jit(solution)/shard_map/all_to_all | solution.py:189
  314.9 0.1 copy.54
  315.0 0.1 mul.289
  315.1 0.1 copy.55
  315.2 50.8 %all-to-all-done.2 = bf16[1,64,8,2048]{3,2,0,1:T(8,128)(2,1)} async-done(((bf16[1,64,8,2048]{3,2,0,1:T(8,128)(2,1)}), bf16[1,64,8,2048]{3,2,0,1:T(8,128)(2,1)}, u32[]{:S(2)}, u32[]{:S(2)}) %all-to-all-start.2) | async-done | bytes 2097184 | tf_op jit(solution)/shard_map/all_to_all | solution.py:189
  366.1 5.2 %gather_fusion.1 = bf16[256,2048]{1,0:T(8,128)(2,1)} fusion(bf16[512,2048]{1,0:T(8,128)(2,1)} %bitcast.37, s32[1024]{0:T(1024)S(1)} %pad_clamp_fusion), kind=kCustom, calls=%fused_computation.1 | custom fusion | bytes 2098176 | tf_op jit(solution)/shard_map/gather | solution.py:190
  371.3 2.7 reshape.683
  374.0 3.2 multiply_reduce_fusion
  377.2 0.8 add_convert_fusion
  (36 shorter events, 0.3 us)
Async XLA Ops:
  6.5 198.3 %copy-start = (bf16[1,512,2048]{2,1,0:T(8,128)(2,1)S(1)}, bf16[1,512,2048]{2,1,0:T(8,128)(2,1)}, u32[]{:S(2)}) copy-start(bf16[1,512,2048]{2,1,0:T(8,128)(2,1)} %param.31) | copy-start | bytes 6291460
  6.5 19.1 %copy-start.2 = (bf16[256,64]{0,1:T(8,128)(2,1)S(1)}, bf16[256,64]{0,1:T(8,128)(2,1)}, u32[]{:S(2)}) copy-start(bf16[256,64]{0,1:T(8,128)(2,1)} %param.19) | copy-start | bytes 98308
  6.5 18.5 %copy-start.6 = (f32[64]{0:T(128)S(1)}, f32[64]{0:T(128)}, u32[]{:S(2)}) copy-start(f32[64]{0:T(128)} %param.21) | copy-start | bytes 772
  6.5 18.7 %copy-start.7 = (f32[4]{0:T(128)S(1)}, f32[4]{0:T(128)}, u32[]{:S(2)}) copy-start(f32[4]{0:T(128)} %param.23) | copy-start | bytes 52
  9.3 16.3 %collective-permute-start = (bf16[128,128]{0,1:T(8,128)(2,1)S(1)}, bf16[128,128]{0,1:T(8,128)(2,1)S(1)}, u32[]{:S(2)}, u32[]{:S(2)}) collective-permute-start(bf16[128,128]{0,1:T(8,128)(2,1)S(1)} %get-tuple-element.11), channel_id=1, source_target_pairs={{0,4},{4,8},{8,12},{12,16},{16,20},{20,24},{24,28},{28,32},{32,36}... | collective-permute-start | bytes 98312 | tf_op jit(solution)/shard_map/ppermute | solution.py:22
  11.3 14.4 %collective-permute-start.1 = (bf16[128,128]{0,1:T(8,128)(2,1)S(1)}, bf16[128,128]{0,1:T(8,128)(2,1)S(1)}, u32[]{:S(2)}, u32[]{:S(2)}) collective-permute-start(bf16[128,128]{0,1:T(8,128)(2,1)S(1)} %get-tuple-element.12), channel_id=1, source_target_pairs={{4,0},{8,4},{12,8},{16,12},{20,16},{24,20},{28,24},{32,28},{36,32}... | collective-permute-start | bytes 98312 | tf_op jit(solution)/shard_map/ppermute | solution.py:23
  15.6 9.8 %collective-permute-start.2 = (bf16[128]{0:T(256)(128)(2,1)S(1)}, bf16[128]{0:T(256)(128)(2,1)S(1)}, u32[]{:S(2)}, u32[]{:S(2)}) collective-permute-start(bf16[128]{0:T(256)(128)(2,1)S(1)} %get-tuple-element.15), channel_id=1, source_target_pairs={{0,4},{4,8},{8,12},{12,16},{16,20},{20,24},{24,28},{28,32},{32,36}... | collective-permute-start | bytes 776 | tf_op jit(solution)/shard_map/ppermute | solution.py:22
  17.5 7.8 %collective-permute-start.3 = (bf16[128]{0:T(256)(128)(2,1)S(1)}, bf16[128]{0:T(256)(128)(2,1)S(1)}, u32[]{:S(2)}, u32[]{:S(2)}) collective-permute-start(bf16[128]{0:T(256)(128)(2,1)S(1)} %get-tuple-element.16), channel_id=1, source_target_pairs={{4,0},{8,4},{12,8},{16,12},{20,16},{24,20},{28,24},{32,28},{36,32}... | collective-permute-start | bytes 776 | tf_op jit(solution)/shard_map/ppermute | solution.py:23
  27.1 11.5 %copy-start.1 = (bf16[64,2048]{1,0:T(8,128)(2,1)S(1)}, bf16[64,2048]{1,0:T(8,128)(2,1)}, u32[]{:S(2)}) copy-start(bf16[64,2048]{1,0:T(8,128)(2,1)} %param.16) | copy-start | bytes 786436
  27.1 11.5 %copy-start.4 = (f32[1024]{0:T(1024)S(1)}, f32[1024]{0:T(1024)}, u32[]{:S(2)}) copy-start(f32[1024]{0:T(1024)} %param.24) | copy-start | bytes 12292
  28.1 10.3 %all-to-all-start = ((bf16[4,64,256]{2,1,0:T(8,128)(2,1)}), bf16[4,64,256]{2,1,0:T(8,128)(2,1)S(1)}, u32[]{:S(2)}, u32[]{:S(2)}) async-start(bf16[4,64,256]{2,1,0:T(8,128)(2,1)} %copy.60), calls=%async_computation | async-start | bytes 262144 | tf_op jit(solution)/shard_map/all_to_all | solution.py:162
  32.4 162.1 %all-gather.3.cloned.1.call-start = ((), (), s32[]{:S(2)}) async-start(), calls=%async_computation.5 | async-start | bytes 10485760 | tf_op jit(solution)/shard_map/all_gather | solution.py:38
  38.5 3.2 copy-start.3
  114.3 189.7 %reduce-scatter.2.cloned.1.call-start = ((), (), s32[]{:S(2)}) async-start(), calls=%async_computation.4 | async-start | bytes 10485760 | tf_op jit(solution)/shard_map/reduce_scatter | solution.py:187
  304.0 11.1 %copy-start.5 = (f32[64,4]{0,1:T(4,128)S(1)}, f32[64,4]{0,1:T(4,128)}, u32[]{:S(2)}) copy-start(f32[64,4]{0,1:T(4,128)} %param.28) | copy-start | bytes 3076
  304.0 62.0 %all-to-all-start.2 = ((bf16[1,64,8,2048]{3,2,0,1:T(8,128)(2,1)}), bf16[1,64,8,2048]{3,2,0,1:T(8,128)(2,1)}, u32[]{:S(2)}, u32[]{:S(2)}) async-start(bf16[1,64,8,2048]{3,2,0,1:T(8,128)(2,1)} %bitcast.102), calls=%async_computation.3 | async-start | bytes 4194304 | tf_op jit(solution)/shard_map/all_to_all | solution.py:189
Sparse Core Ops, SparseCore 0:
  114.5 79.9 all-gather.2
  219.9 84.0 reduce-scatter.1
where the time goes:
time: 386 us; the launch traced here: 385 us
  waiting for transfers between devices  221 us (57%)
  blocking collectives  67.3 us (17%)
  matrix products  29.8 us (8%)
  starting transfers between devices  26.5 us (7%)
  local copies, waits for them, and re-layouts  14.4 us (4%)
  between operations  13.8 us (4%)
  other arithmetic  12.1 us (3%)
    reduce_scatter x1, waiting for transfers between devices, per_device(): lax.psum_scatter(terms.astype(jnp.bfloat16), 'tp', scatter_dimension=0, t...  84.2 us
    all_gather x1, waiting for transfers between devices, piecewise(): parts = [lax.all_gather(section, axis) for section in pieces]  79.9 us
    all_to_all x1, blocking collectives, per_device(): lax.all_to_all(outgoing, 'sp', split_axis=1, concat_axis=1, tiled=True)  67.3 us
    all_to_all x1, waiting for transfers between devices, per_device(): lax.all_to_all(summed, 'sp', split_axis=1, concat_axis=1, tiled=True)  50.8 us
    dot_general x1, matrix products, expert_partial(): jnp.einsum('recf,efd->recd', hidden, w_down, preferred_element_type=jnp.f...  14.9 us
    all_to_all x1, starting transfers between devices, per_device(): lax.all_to_all(summed, 'sp', split_axis=1, concat_axis=1, tiled=True)  10.9 us
    dot_general x1, matrix products, expert_partial(): jnp.einsum('recd,edf->recf', grouped, w_up, preferred_element_type=jnp.fl...  10.4 us
  transfers between devices with their start and end apart: 8, of which 4 were waited for; matrix products, arithmetic and copies ran while one was open for 1% of the time, Pallas kernels for 0%

commit v1 on v0

v1 whole, which is shorter than its diff:
```python
import jax
import jax.numpy as jnp
from jax import lax
from jax.experimental import pallas as pl
from jax.experimental.pallas import tpu as pltpu
from jax.sharding import PartitionSpec as P

WINDOW = 128
MESH = pl.DeviceIdType.MESH

NZ = 8
PLANE = 8
NX = 4
CAP = 8
CHUNKS = 8
WIDE = ()


rope_base = 10000.0
norm_eps = 1e-06
swiglu_limit = 7.0
swiglu_alpha = 1.702
VMEM_LIMIT = 63 * 1024 * 1024


def extended(x, sides, width):
    for axis, dim in sides:
        peers, length = (lax.axis_size(axis), x.shape[dim])
        up = [(i, (i + 1) % peers) for i in range(peers - 1)]
        down = [(j, i) for i, j in up]
        last = lax.slice_in_dim(x, length - width, length, axis=dim)
        leading = lax.slice_in_dim(x, 0, width, axis=dim)
        before = lax.ppermute(last, axis, up)
        after = lax.ppermute(leading, axis, down)
        x = jnp.concatenate([before, x, after], axis=dim)
    return x


def row_normalize(values, gain_vec):
    floats = values.astype(jnp.float32)
    scale_inv = lax.rsqrt(jnp.mean(floats * floats, axis=-1, keepdims=True) + norm_eps)
    return floats * scale_inv * gain_vec


def apply_rotary_heads(heads, token_positions):
    half_size = heads.shape[-1] // 2
    freqs = rope_base ** (-jnp.arange(half_size, dtype=jnp.float32) / half_size)
    angles = token_positions[:, None] * freqs[None, :]
    cosine = jnp.cos(angles)[:, None, :]
    sine = jnp.sin(angles)[:, None, :]
    first_half = heads[..., :half_size]
    second_half = heads[..., half_size:]
    return jnp.concatenate(
        [first_half * cosine - second_half * sine, first_half * sine + second_half * cosine],
        axis=-1,
    )


class Net:
    def __init__(self, sems):
        self.sems = sems
        self.used = 0
        self.copies = {}

    def send(self, name, src, dst, device):
        copy = pltpu.make_async_remote_copy(
            src_ref=src,
            dst_ref=dst,
            send_sem=self.sems.at[self.used],
            recv_sem=self.sems.at[self.used + 1],
            device_id=device,
            device_id_type=MESH,
        )
        self.used += 2
        copy.start()
        self.copies[name] = [copy, False]

    def arrived(self, name):
        self.copies[name][0].wait_recv()

    def sent(self, name):
        if not self.copies[name][1]:
            self.copies[name][0].wait_send()
            self.copies[name][1] = True


def moe_kernel(
    tok_ref, meta_ref, mid_ref, wg_hbm, wu_hbm, wd_hbm, out_ref,
    wg, wu, wd, rows, gate_acc, up_acc, hidden, meta, pick, mix_hi, mix_lo,
    scr_narrow, scr_wide, sems, wsem,
):
    bf16, f32 = jnp.bfloat16, jnp.float32
    width = tok_ref.shape[1] // CHUNKS
    toks = tok_ref.shape[0]
    block = PLANE * toks
    half = block // 2
    sp, x = lax.axis_index("sp"), lax.axis_index("tp")
    z, p = sp // PLANE, lax.rem(sp, PLANE)
    z_up = lax.rem(z + 1, NZ) * PLANE + p
    z_down = lax.rem(z + NZ - 1, NZ) * PLANE + p
    x_up, x_down, x_far = lax.rem(x + 1, NX), lax.rem(x + NX - 1, NX), lax.rem(x + 2, NX)
    up, down = (z_up, x), (z_down, x)
    right, left, far = (sp, x_up), (sp, x_down), (sp, x_far)
    ahead = [(z * PLANE + lax.rem(p + q, PLANE), x) for q in range(PLANE)]
    behind = [(z * PLANE + lax.rem(p + PLANE - q, PLANE), x) for q in range(PLANE)]
    net = Net(sems)
    narrow = [k for k in range(CHUNKS) if k not in WIDE]
    place = {k: (scr_wide, WIDE.index(k), NX) if k in WIDE else (scr_narrow, narrow.index(k), 1) for k in range(CHUNKS)}

    def buf(k, name):
        group, i, _ = place[k]
        return group[name].at[i]

    def cols(k):
        return slice(k * width, (k + 1) * width)

    weight_copies = [
        pltpu.make_async_copy(src.at[0], dst, wsem.at[i])
        for i, (src, dst) in enumerate(((wg_hbm, wg), (wu_hbm, wu), (wd_hbm, wd)))
    ]
    for copy in weight_copies:
        copy.start()

    barrier = pltpu.get_barrier_semaphore()
    peers = [up, down, right, left] + ahead[1:] + ([far] if WIDE else [])
    for peer in peers:
        pl.semaphore_signal(barrier, inc=1, device_id=peer, device_id_type=MESH)
    pl.semaphore_wait(barrier, len(peers))

    meta_width = NX if WIDE else 1

    def up_hops(k):
        return 4 if k % 2 == 0 else 3

    def up_slot(h):
        return h

    def down_slot(h):
        return 4 if h == 4 else (0 if h == 0 else 4 + h)

    def own_tokens(k):
        spread = buf(k, "spread")
        spread[0, 0] = tok_ref[:, cols(k)]

    def wide_first(k):
        spread = buf(k, "spread")
        src = tok_ref.at[:, cols(k)]
        net.send((k, "w", 1), src, spread.at[0, 1], right)
        net.send((k, "w", 2), src, spread.at[0, 2], left)
        net.send((k, "w", 3), src, spread.at[0, 3], far)

    def meta_first():
        meta[0, 0] = meta_ref[...]
        if WIDE:
            net.send(("mw", 1), meta_ref, meta.at[0, 1], right)
            net.send(("mw", 2), meta_ref, meta.at[0, 2], left)
            net.send(("mw", 3), meta_ref, meta.at[0, 3], far)

    def ring_hop(name, h, last_up, last_down, data):
        if h <= last_up:
            if h > 1:
                net.arrived((name, "u", h - 1))
            net.send((name, "u", h), data.at[up_slot(h - 1)], data.at[up_slot(h)], up)
        if h <= last_down:
            if h > 1:
                net.arrived((name, "d", h - 1))
            net.send((name, "d", h), data.at[down_slot(h - 1)], data.at[down_slot(h)], down)

    def meta_hop(h):
        if h == 1 and WIDE:
            for i in (1, 2, 3):
                net.arrived(("mw", i))
        ring_hop("m", h, 4, 3, meta)

    def token_hop(k, h):
        if h == 1 and k in WIDE:
            for i in (1, 2, 3):
                net.arrived((k, "w", i))
        ring_hop(k, h, up_hops(k), 7 - up_hops(k), buf(k, "spread"))

    def tables():
        net.arrived(("m", "u", 4))
        net.arrived(("m", "d", 3))
        shape = (2 * toks, 2 * toks)
        row = lax.broadcasted_iota(jnp.int32, shape, 0)
        lane = lax.broadcasted_iota(jnp.int32, shape, 1)
        expert = z * PLANE + lax.rem(p + row // 16, PLANE)
        target = (expert * CAP + lax.rem(row, CAP)).astype(f32)
        second = lane >= toks
        valid = (lax.rem(row // CAP, 2) == 1) == second
        low = lax.broadcasted_iota(jnp.int32, (16, 2 * toks), 1) < toks
        for xi in range(meta_width):
            for i in range(NZ // 2):
                both = jnp.where(low, meta[2 * i, xi], meta[2 * i + 1, xi])
                chosen = jnp.zeros(shape, f32)
                weighted = jnp.zeros(shape, f32)
                for r in range(4):
                    hit = (both[r : r + 1, :] == target) & valid
                    chosen = jnp.where(hit, 1.0, chosen)
                    weighted = jnp.where(hit, both[8 + r : 9 + r, :], weighted)
                pick[xi, i] = chosen.astype(bf16)
                mixed = weighted.T
                high = mixed.astype(bf16)
                mix_hi[xi, i] = high
                mix_lo[xi, i] = (mixed - high.astype(f32)).astype(bf16)

    def select(k):
        net.arrived((k, "u", up_hops(k)))
        net.arrived((k, "d", 7 - up_hops(k)))
        spread, chosen = buf(k, "spread"), buf(k, "chosen")
        for xi in range(place[k][2]):
            for i in range(NZ // 2):
                pair = jnp.concatenate([spread[2 * i, xi], spread[2 * i + 1, xi]], axis=0)
                got = jnp.dot(pick[xi, i], pair, preferred_element_type=f32).astype(bf16)
                rows[k, xi, 16 * i : 16 * i + 16, :] = got[0:16]
                for q in range(1, PLANE):
                    chosen[q, xi, 16 * i : 16 * i + 16, :] = got[16 * q : 16 * q + 16]
        for q in range(1, PLANE):
            net.send(
                (k, "y", q), chosen.at[q],
                rows.at[k, pl.ds(0, place[k][2]), pl.ds(q * toks, toks), :], ahead[q],
            )

    def gather_rows(k):
        first, second = pl.ds(0, half), pl.ds(half, half)
        for q in range(1, PLANE // 2):
            net.arrived((k, "y", q))
        net.send((k, "rA"), rows.at[k, 0, first, :], rows.at[k, 1, first, :], right)
        for q in range(PLANE // 2, PLANE):
            net.arrived((k, "y", q))
        net.send((k, "lB"), rows.at[k, 0, second, :], rows.at[k, 2, second, :], left)
        net.send((k, "rB"), rows.at[k, 0, second, :], rows.at[k, 1, second, :], right)
        net.send((k, "lA"), rows.at[k, 0, first, :], rows.at[k, 2, first, :], left)

    def forward_rows(k):
        first, second = pl.ds(0, half), pl.ds(half, half)
        net.arrived((k, "rA"))
        net.send((k, "fA"), rows.at[k, 1, first, :], rows.at[k, 3, first, :], right)
        net.arrived((k, "lB"))
        net.send((k, "fB"), rows.at[k, 2, second, :], rows.at[k, 3, second, :], left)

    def expert_in(k, first, last):
        if k in WIDE:
            for q in range(1, PLANE):
                net.arrived((k, "y", q))
        else:
            for name in ("rB", "lA", "fA", "fB"):
                net.arrived((k, name))
        if first:
            weight_copies[0].wait()
            weight_copies[1].wait()

        def tile(i, _):
            xi, part = i // 2, lax.rem(i, 2)
            a = rows[k, xi, pl.ds(pl.multiple_of(part * half, half), half), :]
            at = pl.ds(pl.multiple_of(i * half, half), half)
            g = jnp.dot(a, wg[cols(k), :], preferred_element_type=f32)
            u = jnp.dot(a, wu[cols(k), :], preferred_element_type=f32)
            if not first:
                g = g + gate_acc[at, :]
                u = u + up_acc[at, :]
            if last:
                c = jnp.minimum(g, swiglu_limit)
                u = jnp.clip(u, -swiglu_limit, swiglu_limit)
                hidden[at, :] = ((u + 1.0) * c * jax.nn.sigmoid(swiglu_alpha * c)).astype(bf16)
            else:
                gate_acc[at, :] = g
                up_acc[at, :] = u
            return 0

        lax.fori_loop(0, 2 * NX, tile, 0)

    def expert_out(k, first):
        if first:
            weight_copies[2].wait()
        for q in range(1, PLANE):
            net.sent((k, "y", q))
        if k not in WIDE:
            for name in ("rA", "lB", "rB", "lA", "fA", "fB"):
                net.sent((k, name))

        def tile(i, _):
            xi, part = i // 2, lax.rem(i, 2)
            at = pl.ds(pl.multiple_of(i * half, half), half)
            made = jnp.dot(hidden[at, :], wd[:, cols(k)], preferred_element_type=f32)
            rows[k, xi, pl.ds(pl.multiple_of(part * half, half), half), :] = made.astype(bf16)
            return 0

        lax.fori_loop(0, 2 * NX, tile, 0)
        a, b = pl.ds(0, half), pl.ds(half, half)
        if k in WIDE:
            back = buf(k, "back")
            for q in range(1, PLANE):
                net.send((k, "b", q), rows.at[k, pl.ds(0, NX), pl.ds(q * toks, toks), :], back.at[q], behind[q])
        else:
            net.send((k, "oA"), rows.at[k, 3, a, :], buf(k, "hop_r"), right)
            net.send((k, "oB"), rows.at[k, 3, b, :], buf(k, "hop_l"), left)
            net.send((k, "dB"), rows.at[k, 2, b, :], buf(k, "sum_r").at[b, :], right)
            net.send((k, "dA"), rows.at[k, 1, a, :], buf(k, "sum_l").at[a, :], left)

    def reduce_hop(k):
        a, b = pl.ds(0, half), pl.ds(half, half)
        net.arrived((k, "oA"))
        rows[k, 2, a, :] = (rows[k, 2, a, :].astype(f32) + buf(k, "hop_r")[...].astype(f32)).astype(bf16)
        net.send((k, "sA"), rows.at[k, 2, a, :], buf(k, "sum_r").at[a, :], right)
        net.arrived((k, "oB"))
        rows[k, 1, b, :] = (rows[k, 1, b, :].astype(f32) + buf(k, "hop_l")[...].astype(f32)).astype(bf16)
        net.send((k, "sB"), rows.at[k, 1, b, :], buf(k, "sum_l").at[b, :], left)

    def reduce_rows(k):
        for name in ("dB", "dA", "sA", "sB"):
            net.arrived((k, name))
        back, total = buf(k, "back"), buf(k, "total")
        total[...] = (
            rows[k, 0].astype(f32) + buf(k, "sum_r")[...].astype(f32) + buf(k, "sum_l")[...].astype(f32)
        ).astype(bf16)
        for q in range(1, PLANE):
            net.send((k, "b", q), total.at[pl.ds(q * toks, toks), :], back.at[q, 0], behind[q])

    def combine(k):
        for q in range(1, PLANE):
            net.arrived((k, "b", q))
        back, mixed = buf(k, "back"), buf(k, "mixed")
        for xi in range(place[k][2]):
            for i in range(NZ // 2):
                part = slice(16 * i, 16 * i + 16)
                own = rows[k, xi, part, :] if k in WIDE else buf(k, "total")[part, :]
                outs = jnp.concatenate([own] + [back[q, xi, part, :] for q in range(1, PLANE)], axis=0)
                got = jnp.dot(mix_hi[xi, i], outs, preferred_element_type=f32)
                got = got + jnp.dot(mix_lo[xi, i], outs, preferred_element_type=f32)
                mixed[2 * i, xi] = got[:toks]
                mixed[2 * i + 1, xi] = got[toks:]

    def return_hop(k, h):
        mixed, leaving = buf(k, "mixed"), buf(k, "leaving")
        for way, hops, slot, landing, to in (
            ("D", up_hops(k), up_slot, buf(k, "from_up"), down),
            ("U", 7 - up_hops(k), down_slot, buf(k, "from_down"), up),
        ):
            j = hops - h + 1
            if j < 1:
                continue
            value = mixed[slot(j)]
            if h > 1:
                net.arrived((k, way, h - 1))
                value = value + landing[j].astype(f32)
            leaving[slot(j)] = value.astype(bf16)
            net.send((k, way, h), leaving.at[slot(j)], landing.at[j - 1], to)

    def finish(k):
        mixed = buf(k, "mixed")
        net.arrived((k, "D", up_hops(k)))
        net.arrived((k, "U", 7 - up_hops(k)))
        value = mixed[0] + buf(k, "from_up")[0].astype(f32) + buf(k, "from_down")[0].astype(f32)
        if k in WIDE:
            mixed[0] = value
            leaving = buf(k, "leaving")
            leaving[0] = value.astype(bf16)
            last = buf(k, "last")
            net.send((k, "X", 2), leaving.at[0, 2], last.at[2], right)
            net.send((k, "X", 1), leaving.at[0, 1], last.at[1], left)
            net.send((k, "X", 3), leaving.at[0, 3], last.at[3], far)
        else:
            out_ref[:, cols(k)] = (mid_ref[:, cols(k)].astype(f32) + value[0]).astype(bf16)

    def finish_wide(k):
        mixed, last = buf(k, "mixed"), buf(k, "last")
        value = mixed[0, 0]
        for i in (1, 2, 3):
            net.arrived((k, "X", i))
            value = value + last[i].astype(f32)
        out_ref[:, cols(k)] = (mid_ref[:, cols(k)].astype(f32) + value).astype(bf16)

    def run(steps):
        for _, _, step, args in sorted(steps, key=lambda s: s[:2]):
            step(*args)

    meta_first()
    for k in WIDE:
        wide_first(k)
    for k in range(CHUNKS):
        own_tokens(k)
    for h in range(1, 2):
        meta_hop(h)
    order = narrow + list(WIDE)
    steps = []
    for h in range(2, 5):
        steps.append((h - 1, 0, meta_hop, (h,)))
    steps.append((4, 4.5, tables, ()))
    for t, k in enumerate(order):
        for h in range(1, 5):
            steps.append((t + h - 1, 5 - h, token_hop, (k, h)))
        steps.append((t + 4, 5, select, (k,)))
        if k not in WIDE:
            steps.append((t + 5, 6, gather_rows, (k,)))
            steps.append((t + 7, 7, forward_rows, (k,)))
        steps.append((t + 9, 8, expert_in, (k, t == 0, t == CHUNKS - 1)))
    run(steps)

    order = list(WIDE) + narrow
    steps = []
    for t, k in enumerate(order):
        steps.append((t, 5, expert_out, (k, t == 0)))
        if k not in WIDE:
            steps.append((t + 1, 6, reduce_hop, (k,)))
            steps.append((t + 3, 7, reduce_rows, (k,)))
        steps.append((t + 4, 8, combine, (k,)))
        for h in range(1, 5):
            steps.append((t + 4 + h, 5 - h, return_hop, (k, h)))
        steps.append((t + 9, 0, finish, (k,)))
        if k in WIDE:
            steps.append((t + 11, 0.5, finish_wide, (k,)))
    run(steps)
    for name in net.copies:
        net.sent(name)
    assert net.used == sems.shape[0], net.used


def moe(tokens, meta, middle, w_gate, w_up, w_down):
    bf16, f32 = jnp.bfloat16, jnp.float32
    toks, model = tokens.shape
    width = model // CHUNKS
    units = w_gate.shape[2]
    block = PLANE * toks
    wides = len(WIDE)
    meta_width = NX if WIDE else 1

    def group(count, nx):
        if count == 0:
            return {"none": pltpu.VMEM((16, 128), bf16)}
        shapes = {
            "spread": pltpu.VMEM((count, NZ, nx, toks, width), bf16),
            "chosen": pltpu.VMEM((count, PLANE, nx, toks, width), bf16),
            "back": pltpu.VMEM((count, PLANE, nx, toks, width), bf16),
            "mixed": pltpu.VMEM((count, NZ, nx, toks, width), f32),
            "leaving": pltpu.VMEM((count, NZ, nx, toks, width), bf16),
            "from_up": pltpu.VMEM((count, 4, nx, toks, width), bf16),
            "from_down": pltpu.VMEM((count, 4, nx, toks, width), bf16),
        }
        if nx == 1:
            shapes["hop_r"] = pltpu.VMEM((count, block // 2, width), bf16)
            shapes["hop_l"] = pltpu.VMEM((count, block // 2, width), bf16)
            shapes["sum_r"] = pltpu.VMEM((count, block, width), bf16)
            shapes["sum_l"] = pltpu.VMEM((count, block, width), bf16)
            shapes["total"] = pltpu.VMEM((count, block, width), bf16)
        else:
            shapes["last"] = pltpu.VMEM((count, nx, toks, width), bf16)
        return shapes

    per_narrow = 7 + 7 + 6 + 6 + 7 + 7
    per_wide = 3 + 7 + 7 + 7 + 7 + 3
    copies = 7 + (3 if WIDE else 0) + (CHUNKS - wides) * per_narrow + wides * per_wide
    any_spec = pl.BlockSpec(memory_space=pl.ANY)
    vmem_spec = pl.BlockSpec(memory_space=pltpu.VMEM)
    narrow_shapes, wide_shapes = group(CHUNKS - wides, 1), group(wides, NX)
    names_n, names_w = list(narrow_shapes), list(wide_shapes)

    def body(*refs):
        fixed, rest = refs[:18], refs[18:]
        scr_n = dict(zip(names_n, rest[: len(names_n)]))
        rest = rest[len(names_n) :]
        scr_w = dict(zip(names_w, rest[: len(names_w)]))
        sems, wsem = rest[len(names_w) :]
        moe_kernel(*fixed, scr_n, scr_w, sems, wsem)

    tables = [pltpu.VMEM((meta_width, NZ // 2, 2 * toks, 2 * toks), bf16) for _ in range(3)]
    return pl.pallas_call(
        body,
        out_shape=jax.ShapeDtypeStruct((toks, model), bf16),
        in_specs=[vmem_spec, vmem_spec, vmem_spec, any_spec, any_spec, any_spec],
        out_specs=vmem_spec,
        scratch_shapes=[
            pltpu.VMEM((model, units), bf16),
            pltpu.VMEM((model, units), bf16),
            pltpu.VMEM((units, model), bf16),
            pltpu.VMEM((CHUNKS, NX, block, width), bf16),
            pltpu.VMEM((NX * block, units), f32),
            pltpu.VMEM((NX * block, units), f32),
            pltpu.VMEM((NX * block, units), bf16),
            pltpu.VMEM((NZ, meta_width, 16, 2 * toks), f32),
            *tables,
            *narrow_shapes.values(),
            *wide_shapes.values(),
            pltpu.SemaphoreType.DMA((2 * copies,)),
            pltpu.SemaphoreType.DMA((3,)),
        ],
        compiler_params=pltpu.CompilerParams(
            collective_id=0, has_side_effects=True, vmem_limit_bytes=VMEM_LIMIT
        ),
        name="experts",
    )(tokens, meta, middle, w_gate, w_up, w_down)


def route_table(own_routes, weights):
    routes = own_routes.T
    top, toks = routes.shape
    ids = jnp.arange(toks, dtype=jnp.int32)
    same = routes[:, :, None, None] == routes[None, None, :, :]
    earlier = ids[None, None, None, :] < ids[None, :, None, None]
    rank = jnp.sum((same & earlier).astype(jnp.int32), axis=(2, 3))
    slots = (routes * CAP + rank).astype(jnp.float32)
    pad = jnp.full((8 - top, toks), -1.0, jnp.float32)
    table = jnp.concatenate([slots, pad, weights.T, pad], axis=0)
    return jnp.concatenate([table, table], axis=1)


def per_device(
    resid,
    queries,
    keys,
    values,
    docs,
    q_gain,
    key_norm_gain,
    sink,
    out_gain,
    w_out,
    norm_gain,
    routes,
    route_weights,
    w_gate,
    w_up,
    w_down,
):
    tp_size = lax.axis_size("tp")
    sp_index = lax.axis_index("sp")
    tp_index = lax.axis_index("tp")
    tok_rows = queries.shape[0]
    head_size = q_gain.shape[0]
    query_heads = sink.shape[0]
    kv_heads = keys.shape[1] // head_size
    query_group_width = query_heads // kv_heads
    token_positions = (sp_index * tok_rows + jnp.arange(tok_rows, dtype=jnp.int32)).astype(
        jnp.float32
    )
    q_rot = apply_rotary_heads(
        row_normalize(queries.reshape(tok_rows, query_heads, head_size), q_gain), token_positions
    ).astype(jnp.bfloat16)
    key_rotated = apply_rotary_heads(
        row_normalize(keys.reshape(tok_rows, kv_heads, head_size), key_norm_gain), token_positions
    ).astype(jnp.bfloat16)
    key_value = jnp.concatenate(
        [key_rotated.reshape(tok_rows, kv_heads * head_size), values], axis=1
    )
    doc_mark = (docs + 1).astype(jnp.bfloat16)
    kv_span, doc_span = (
        extended(key_value, (("sp", 0),), WINDOW),
        extended(doc_mark, (("sp", 0),), WINDOW),
    )
    span_rows = tok_rows + 2 * WINDOW
    k_span = kv_span[:, : kv_heads * head_size].reshape(span_rows, kv_heads, head_size)
    v_span = kv_span[:, kv_heads * head_size :].reshape(span_rows, kv_heads, head_size)
    scores = jnp.einsum(
        "qhgd,khd->hgqk",
        q_rot.reshape(tok_rows, kv_heads, query_group_width, head_size),
        k_span,
        preferred_element_type=jnp.float32,
    ) * head_size ** (-0.5)
    offsets = jnp.arange(tok_rows, dtype=jnp.int32)[:, None] - (
        jnp.arange(span_rows, dtype=jnp.int32)[None, :] - WINDOW
    )
    allowed = (jnp.abs(offsets) <= WINDOW) & (doc_mark[:, None] == doc_span[None, :])
    raw_weights = jnp.where(allowed[None, None], jnp.exp(scores), jnp.zeros((), jnp.float32))
    sink_exponent = jnp.exp(sink).reshape(kv_heads, query_group_width)
    total = jnp.sum(raw_weights, axis=-1) + sink_exponent[:, :, None]
    probs = (raw_weights / total[..., None]).astype(jnp.bfloat16)
    att = jnp.einsum("hgqk,khd->qhgd", probs, v_span, preferred_element_type=jnp.float32)
    att = att.astype(jnp.bfloat16).reshape(tok_rows, query_heads * head_size)
    by_token = lax.all_to_all(att, "tp", split_axis=0, concat_axis=1, tiled=True)
    att_normed = row_normalize(by_token, out_gain).astype(jnp.bfloat16)
    middle = (
        resid.astype(jnp.float32) + jnp.dot(att_normed, w_out, preferred_element_type=jnp.float32)
    ).astype(jnp.bfloat16)
    moe_in = row_normalize(middle, norm_gain).astype(jnp.bfloat16)
    quarter = tok_rows // tp_size
    own_routes = lax.dynamic_slice_in_dim(routes, tp_index * quarter, quarter, 0)
    table = route_table(own_routes, route_weights)
    return moe(moe_in, table, middle, w_gate, w_up, w_down)


def solution(mesh):
    return jax.shard_map(
        per_device,
        mesh=mesh,
        in_specs=(
            P(("sp", "tp"), None),
            P("sp", "tp"),
            P("sp", "tp"),
            P("sp", "tp"),
            P("sp"),
            P(),
            P(),
            P("tp"),
            P(),
            P(),
            P(),
            P("sp", None),
            P(("sp", "tp"), None),
            P("sp", None, "tp"),
            P("sp", None, "tp"),
            P("sp", "tp", None),
        ),
        out_specs=P(("sp", "tp"), None),
        check_vma=False,
    )
```

time: 386 us -> 245 us (0.63)
  waiting for transfers between devices: 221 us -> 5.31 us
  Pallas kernels: 0 us -> 206 us
  blocking collectives: 67.3 us -> 0 us
  matrix products: 29.8 us -> 4.5 us
  between operations: 13.8 us -> 0.29 us
  starting transfers between devices: 26.5 us -> 15.4 us
  local copies, waits for them, and re-layouts: 14.4 us -> 4.48 us
  other arithmetic: 12.1 us -> 7.36 us
    pallas_call x0 -> x1, Pallas kernels: none -> 206 us  [moe(): pl.pallas_call(body, out_shape=jax.ShapeDtypeStruct((toks, model), bf16),...]
    reduce_scatter x1 -> x0, waiting for transfers between devices: 84.2 us -> none  [per_device(): lax.psum_scatter(terms.astype(jnp.bfloat16), 'tp', scatter_dimension=0, t...]
    all_gather x1 -> x0, waiting for transfers between devices: 79.9 us -> none  [piecewise(): parts = [lax.all_gather(section, axis) for section in pieces]]
    all_to_all x1 -> x0, blocking collectives: 67.3 us -> none  [per_device(): lax.all_to_all(outgoing, 'sp', split_axis=1, concat_axis=1, tiled=True)]
    all_to_all x1 -> x0, waiting for transfers between devices: 50.8 us -> none  [per_device(): lax.all_to_all(summed, 'sp', split_axis=1, concat_axis=1, tiled=True)]
    dot_general x2 -> x0, matrix products: 25.3 us -> none  [the longest x1 14.9 us: expert_partial(): jnp.einsum('recf,efd->recd', hidden, w_down, preferred_element_type=jnp.f...]
    all_to_all x1 -> x0, starting transfers between devices: 10.9 us -> none  [per_device(): lax.all_to_all(summed, 'sp', split_axis=1, concat_axis=1, tiled=True)]
    gather x2 -> x0, local copies, waits for them, and re-layouts: 8.55 us -> none  [the longest x1 5.21 us: per_device(): returned.reshape(-1, model_width)[own_slot]]
  transfers between devices with their start and end apart: 8 -> 5, of which waited for: 4 -> 1; matrix products, arithmetic and copies ran while one was open for 1% -> 2% of each run, Pallas kernels for 0% -> 0%
where the time goes in v1:
time: 245 us; the launch traced here: 244 us
  Pallas kernels  206 us (84%)
  starting transfers between devices  15.4 us (6%)
  other arithmetic  7.36 us (3%)
  waiting for transfers between devices  5.31 us (2%)
  matrix products  4.5 us (2%)
  local copies, waits for them, and re-layouts  4.48 us (2%)
    pallas_call x1, Pallas kernels, moe(): pl.pallas_call(body, out_shape=jax.ShapeDtypeStruct((toks, model), bf16),...  206 us
    ppermute x2, starting transfers between devices, extended(): after = lax.ppermute(leading, axis, down)  7.28 us
    all_to_all x1, waiting for transfers between devices, per_device(): lax.all_to_all(att, 'tp', split_axis=0, concat_axis=1, tiled=True)  5.3 us
  transfers between devices with their start and end apart: 5, of which 1 were waited for; matrix products, arithmetic and copies ran while one was open for 2% of the time, Pallas kernels for 0%

profile of v1, /device:TPU:8, one launch (start us, length us, event | category | flops | bytes accessed | tf_op | source)
XLA Modules:
  0.0 243.6 jit_solution(13172524566466804035)
XLA Ops:
  0.0 0.0 copy-start.2
  0.0 0.0 copy-start.6
  0.0 0.8 fusion.15
  0.8 0.8 fusion.17
  1.7 0.2 fusion.27
  1.9 0.8 pad_maximum_fusion.1
  2.6 1.9 collective-permute-start
  4.6 3.6 %collective-permute-start.1 = (bf16[128,128]{0,1:T(8,128)(2,1)S(1)}, bf16[128,128]{0,1:T(8,128)(2,1)S(1)}, u32[]{:S(2)}, u32[]{:S(2)}) collective-permute-start(bf16[128,128]{0,1:T(8,128)(2,1)S(1)} %get-tuple-element.10), channel_id=1, source_target_pairs={{4,0},{8,4},{12,8},{16,12},{20,16},{24,20},{28,24},{32,28},{36,32}... | collective-permute-start | bytes 98312 | tf_op jit(solution)/shard_map/ppermute | solution.py:34
  8.2 0.7 add_convert_fusion.2
  8.9 1.9 collective-permute-start.2
  10.8 3.6 %collective-permute-start.3 = (bf16[128]{0:T(256)(128)(2,1)S(1)}, bf16[128]{0:T(256)(128)(2,1)S(1)}, u32[]{:S(2)}, u32[]{:S(2)}) collective-permute-start(bf16[128]{0:T(256)(128)(2,1)S(1)} %get-tuple-element.14), channel_id=1, source_target_pairs={{4,0},{8,4},{12,8},{16,12},{20,16},{24,20},{28,24},{32,28},{36,32}... | collective-permute-start | bytes 776 | tf_op jit(solution)/shard_map/ppermute | solution.py:34
  14.5 0.2 multiply_cosine_fusion
  14.7 1.0 copy.23
  15.8 0.8 dynamic-slice_bitcast_fusion
  16.5 0.3 convert_reduce_fusion
  16.8 0.8 add_convert_fusion.1
  17.6 0.7 multiply_multiply_fusion
  18.4 0.0 copy-done.6
  18.4 0.0 collective-permute-done.2
  18.4 0.0 collective-permute-done.3
  18.4 0.2 fusion.7
  18.7 0.0 collective-permute-done
  18.7 0.0 collective-permute-done.1
  18.7 0.0 copy-done.2
  18.7 0.7 fusion.1
  19.4 0.1 broadcast_add_fusion
  19.4 0.0 copy-start.5
  19.5 0.6 fusion.2
  20.1 0.0 copy-start.1
  20.1 0.0 copy-start.4
  20.1 0.2 reshape.303
  20.3 0.8 copy.28
  21.1 4.3 %all-to-all-start = ((bf16[4,64,256]{2,1,0:T(8,128)(2,1)}), bf16[4,64,256]{2,1,0:T(8,128)(2,1)S(1)}, u32[]{:S(2)}, u32[]{:S(2)}) async-start(bf16[4,64,256]{2,1,0:T(8,128)(2,1)} %copy.28), calls=%async_computation | async-start | bytes 262144 | tf_op jit(solution)/shard_map/all_to_all | solution.py:569
  25.4 0.0 copy-done.5
  25.4 0.7 maximum_maximum_fusion.refs_1_
  26.1 5.3 %all-to-all-done = bf16[4,64,256]{2,1,0:T(8,128)(2,1)S(1)} async-done(((bf16[4,64,256]{2,1,0:T(8,128)(2,1)}), bf16[4,64,256]{2,1,0:T(8,128)(2,1)S(1)}, u32[]{:S(2)}, u32[]{:S(2)}) %all-to-all-start) | async-done | bytes 131104 | tf_op jit(solution)/shard_map/all_to_all | solution.py:569
  31.4 0.1 fusion.8
  31.5 0.0 copy-done.1
  31.6 0.0 copy-done.4
  31.6 0.0 copy-start.3
  31.6 3.2 %fusion.4 = (f32[64]{0:T(128)S(1)}, bf16[64,2048]{1,0:T(8,128)(2,1)S(1)}) fusion(bf16[1024,2048]{1,0:T(8,128)(2,1)} %param.25, f32[64,1024]{1,0:T(8,128)S(1)} %bitcast.49, f32[1024]{0:T(1024)S(1)} %copy-done.4, f32[64]{0:T(128)S(1)} %add_rsqrt_fusion.3, bf16[64,2048]{1,0:T(8,128)(2,1)S(1)} %copy-done.1), kind=kOutput, calls=%fused_computation.10 | convolution fusion | flops 269418432 | bytes 4985344 | tf_op jit(solution)/shard_map/dot_general | solution.py:572
  34.8 0.0 copy-start
  34.8 0.0 copy-done.3
  34.8 0.8 fusion.6.refs_0_
  35.7 0.0 copy-done
  35.7 206.2 %experts.1 = bf16[64,2048]{1,0:T(8,128)(2,1)} custom-call(bf16[64,2048]{1,0:T(8,128)(2,1)} %fusion.6.refs_0_, f32[16,128]{1,0:T(8,128)} %maximum_maximum_fusion.refs_1_, bf16[64,2048]{1,0:T(8,128)(2,1)} %copy-done, bf16[1,2048,512]{2,1,0:T(8,128)(2,1)} %refs_3_.1, bf16[1,2048,512]{2,1,0:T(8,128)(2,1)} %refs_4_.1, bf16[1,512,2048]{2,1,0:T(8,128)(2,1)} %refs_5_.1), custom_call_target="tpu_custom_call" | custom-call | tf_op jit(solution)/shard_map/experts/pallas_call | solution.py:467
  241.9 1.7 copy.31
  (18 shorter events, 0.2 us)
Async XLA Ops:
  0.0 18.7 %copy-start.2 = (bf16[256,64]{0,1:T(8,128)(2,1)S(1)}, bf16[256,64]{0,1:T(8,128)(2,1)}, u32[]{:S(2)}) copy-start(bf16[256,64]{0,1:T(8,128)(2,1)} %param.19) | copy-start | bytes 98308
  0.0 18.4 %copy-start.6 = (f32[4]{0:T(128)S(1)}, f32[4]{0:T(128)}, u32[]{:S(2)}) copy-start(f32[4]{0:T(128)} %param.23) | copy-start | bytes 52
  2.6 16.0 %collective-permute-start = (bf16[128,128]{0,1:T(8,128)(2,1)S(1)}, bf16[128,128]{0,1:T(8,128)(2,1)S(1)}, u32[]{:S(2)}, u32[]{:S(2)}) collective-permute-start(bf16[128,128]{0,1:T(8,128)(2,1)S(1)} %get-tuple-element.9), channel_id=1, source_target_pairs={{0,4},{4,8},{8,12},{12,16},{16,20},{20,24},{24,28},{28,32},{32,36}... | collective-permute-start | bytes 98312 | tf_op jit(solution)/shard_map/ppermute | solution.py:33
  4.6 14.1 %collective-permute-start.1 = (bf16[128,128]{0,1:T(8,128)(2,1)S(1)}, bf16[128,128]{0,1:T(8,128)(2,1)S(1)}, u32[]{:S(2)}, u32[]{:S(2)}) collective-permute-start(bf16[128,128]{0,1:T(8,128)(2,1)S(1)} %get-tuple-element.10), channel_id=1, source_target_pairs={{4,0},{8,4},{12,8},{16,12},{20,16},{24,20},{28,24},{32,28},{36,32}... | collective-permute-start | bytes 98312 | tf_op jit(solution)/shard_map/ppermute | solution.py:34
  8.9 9.5 %collective-permute-start.2 = (bf16[128]{0:T(256)(128)(2,1)S(1)}, bf16[128]{0:T(256)(128)(2,1)S(1)}, u32[]{:S(2)}, u32[]{:S(2)}) collective-permute-start(bf16[128]{0:T(256)(128)(2,1)S(1)} %get-tuple-element.13), channel_id=1, source_target_pairs={{0,4},{4,8},{8,12},{12,16},{16,20},{20,24},{24,28},{28,32},{32,36}... | collective-permute-start | bytes 776 | tf_op jit(solution)/shard_map/ppermute | solution.py:33
  10.8 7.6 %collective-permute-start.3 = (bf16[128]{0:T(256)(128)(2,1)S(1)}, bf16[128]{0:T(256)(128)(2,1)S(1)}, u32[]{:S(2)}, u32[]{:S(2)}) collective-permute-start(bf16[128]{0:T(256)(128)(2,1)S(1)} %get-tuple-element.14), channel_id=1, source_target_pairs={{4,0},{8,4},{12,8},{16,12},{20,16},{24,20},{28,24},{32,28},{36,32}... | collective-permute-start | bytes 776 | tf_op jit(solution)/shard_map/ppermute | solution.py:34
  19.4 5.9 %copy-start.5 = (f32[64,4]{0,1:T(4,128)S(1)}, f32[64,4]{0,1:T(4,128)}, u32[]{:S(2)}) copy-start(f32[64,4]{0,1:T(4,128)} %param.28) | copy-start | bytes 3076
  20.1 11.5 %copy-start.1 = (bf16[64,2048]{1,0:T(8,128)(2,1)S(1)}, bf16[64,2048]{1,0:T(8,128)(2,1)}, u32[]{:S(2)}) copy-start(bf16[64,2048]{1,0:T(8,128)(2,1)} %param.16) | copy-start | bytes 786436
  20.1 11.5 %copy-start.4 = (f32[1024]{0:T(1024)S(1)}, f32[1024]{0:T(1024)}, u32[]{:S(2)}) copy-start(f32[1024]{0:T(1024)} %param.24) | copy-start | bytes 12292
  21.1 10.3 %all-to-all-start = ((bf16[4,64,256]{2,1,0:T(8,128)(2,1)}), bf16[4,64,256]{2,1,0:T(8,128)(2,1)S(1)}, u32[]{:S(2)}, u32[]{:S(2)}) async-start(bf16[4,64,256]{2,1,0:T(8,128)(2,1)} %copy.28), calls=%async_computation | async-start | bytes 262144 | tf_op jit(solution)/shard_map/all_to_all | solution.py:569
  31.6 3.3 %copy-start.3 = (f32[2048]{0:T(1024)S(1)}, f32[2048]{0:T(1024)}, u32[]{:S(2)}) copy-start(f32[2048]{0:T(1024)} %param.26) | copy-start | bytes 24580
  34.8 0.9 copy-start

commit v2 on v1

--- a/solution.py
+++ b/solution.py
@@ -13,14 +13,29 @@
 NX = 4
 CAP = 8
 CHUNKS = 8
-WIDE = ()
+WIDE = (6, 7)
+VMEM_LIMIT = 63 * 1024 * 1024
+ORDER = (
+    (0,), (1, 1), (5, 1, 1), (5, 0, 1), (4, 6), (1, 2), (5, 1, 2), (5, 4, 1), (1, 3), (5, 1, 3), (5, 0, 2), (1, 4),
+    (5, 1, 4), (5, 4, 2), (4, 7), (5, 0, 3), (3, 0), (6, 1), (5, 3, 1), (5, 5, 1), (5, 2, 1), (5, 0, 4), (5, 4, 3),
+    (5, 3, 2), (5, 5, 2), (5, 2, 2), (7, 1), (5, 4, 4), (6, 0), (5, 7, 1), (5, 3, 3), (5, 2, 3), (8, 1), (6, 4),
+    (2, 1), (5, 5, 3), (7, 0), (5, 3, 4), (5, 7, 2), (6, 3), (2, 2), (7, 4), (5, 2, 4), (5, 5, 4), (8, 0),
+    (5, 7, 3), (8, 4), (6, 2), (6, 5), (2, 3), (5, 6, 1), (7, 3), (5, 7, 4), (2, 4), (7, 2), (5, 6, 2), (3, 1),
+    (6, 7), (5, 6, 3), (5, 6, 4), (7, 5), (9, 1), (8, 3), (9, 4), (6, 6), (9, 7), (8, 2), (8, 5), (9, 0), (9, 3),
+    (9, 2), (9, 5), (9, 6), (10, 6), (10, 7), (10, 0), (10, 1), (11, 1), (11, 0), (10, 2), (13, 6), (14, 6, 1),
+    (10, 3), (14, 6, 2), (12, 1), (13, 7), (12, 0), (14, 7, 1), (14, 6, 3), (14, 7, 2), (11, 2), (11, 3), (10, 4),
+    (12, 2), (13, 1), (14, 1, 1), (14, 7, 3), (14, 1, 2), (13, 0), (14, 6, 4), (11, 4), (14, 0, 1), (12, 3),
+    (10, 5), (13, 2), (14, 2, 1), (14, 1, 3), (14, 7, 4), (12, 4), (14, 1, 4), (14, 0, 2), (11, 5), (14, 2, 2),
+    (15, 7), (13, 3), (14, 3, 1), (15, 1), (14, 2, 3), (13, 4), (12, 5), (14, 4, 1), (14, 3, 2), (15, 6),
+    (14, 0, 3), (14, 3, 3), (14, 4, 2), (13, 5), (14, 5, 1), (14, 4, 3), (14, 5, 2), (14, 0, 4), (14, 5, 3),
+    (14, 4, 4), (14, 2, 4), (14, 3, 4), (15, 0), (14, 5, 4), (16, 6), (16, 7), (15, 4), (15, 3), (15, 2), (15, 5),
+)
 
 
 rope_base = 10000.0
 norm_eps = 1e-06
 swiglu_limit = 7.0
 swiglu_alpha = 1.702
-VMEM_LIMIT = 63 * 1024 * 1024
 
 
 def extended(x, sides, width):
@@ -121,6 +136,10 @@
     for copy in weight_copies:
         copy.start()
 
+    meta[0, 0] = meta_ref[...]
+    for k in range(CHUNKS):
+        buf(k, "spread")[0, 0] = tok_ref[:, cols(k)]
+
     barrier = pltpu.get_barrier_semaphore()
     peers = [up, down, right, left] + ahead[1:] + ([far] if WIDE else [])
     for peer in peers:
@@ -137,10 +156,6 @@
 
     def down_slot(h):
         return 4 if h == 4 else (0 if h == 0 else 4 + h)
-
-    def own_tokens(k):
-        spread = buf(k, "spread")
-        spread[0, 0] = tok_ref[:, cols(k)]
 
     def wide_first(k):
         spread = buf(k, "spread")
@@ -150,7 +165,6 @@
         net.send((k, "w", 3), src, spread.at[0, 3], far)
 
     def meta_first():
-        meta[0, 0] = meta_ref[...]
         if WIDE:
             net.send(("mw", 1), meta_ref, meta.at[0, 1], right)
             net.send(("mw", 2), meta_ref, meta.at[0, 2], left)
@@ -167,10 +181,13 @@
             net.send((name, "d", h), data.at[down_slot(h - 1)], data.at[down_slot(h)], down)
 
     def meta_hop(h):
-        if h == 1 and WIDE:
+        ring_hop("m", h, 4, 3, meta.at[:, 0])
+
+    def meta_wide_hop(h):
+        if h == 1:
             for i in (1, 2, 3):
                 net.arrived(("mw", i))
-        ring_hop("m", h, 4, 3, meta)
+        ring_hop("mz", h, 4, 3, meta.at[:, pl.ds(1, NX - 1)])
 
     def token_hop(k, h):
         if h == 1 and k in WIDE:
@@ -178,9 +195,10 @@
                 net.arrived((k, "w", i))
         ring_hop(k, h, up_hops(k), 7 - up_hops(k), buf(k, "spread"))
 
-    def tables():
-        net.arrived(("m", "u", 4))
-        net.arrived(("m", "d", 3))
+    def tables(others):
+        indices = range(1, NX) if others else (0,)
+        net.arrived(("mz" if others else "m", "u", 4))
+        net.arrived(("mz" if others else "m", "d", 3))
         shape = (2 * toks, 2 * toks)
         row = lax.broadcasted_iota(jnp.int32, shape, 0)
         lane = lax.broadcasted_iota(jnp.int32, shape, 1)
@@ -189,7 +207,7 @@
         second = lane >= toks
         valid = (lax.rem(row // CAP, 2) == 1) == second
         low = lax.broadcasted_iota(jnp.int32, (16, 2 * toks), 1) < toks
-        for xi in range(meta_width):
+        for xi in indices:
             for i in range(NZ // 2):
                 both = jnp.where(low, meta[2 * i, xi], meta[2 * i + 1, xi])
                 chosen = jnp.zeros(shape, f32)
@@ -215,7 +233,7 @@
                 rows[k, xi, 16 * i : 16 * i + 16, :] = got[0:16]
                 for q in range(1, PLANE):
                     chosen[q, xi, 16 * i : 16 * i + 16, :] = got[16 * q : 16 * q + 16]
-        for q in range(1, PLANE):
+        for q in (4, 5, 2, 3, 6, 7, 1):
             net.send(
                 (k, "y", q), chosen.at[q],
                 rows.at[k, pl.ds(0, place[k][2]), pl.ds(q * toks, toks), :], ahead[q],
@@ -290,7 +308,7 @@
         a, b = pl.ds(0, half), pl.ds(half, half)
         if k in WIDE:
             back = buf(k, "back")
-            for q in range(1, PLANE):
+            for q in (4, 5, 2, 3, 6, 7, 1):
                 net.send((k, "b", q), rows.at[k, pl.ds(0, NX), pl.ds(q * toks, toks), :], back.at[q], behind[q])
         else:
             net.send((k, "oA"), rows.at[k, 3, a, :], buf(k, "hop_r"), right)
@@ -314,7 +332,7 @@
         total[...] = (
             rows[k, 0].astype(f32) + buf(k, "sum_r")[...].astype(f32) + buf(k, "sum_l")[...].astype(f32)
         ).astype(bf16)
-        for q in range(1, PLANE):
+        for q in (4, 5, 2, 3, 6, 7, 1):
             net.send((k, "b", q), total.at[pl.ds(q * toks, toks), :], back.at[q, 0], behind[q])
 
     def combine(k):
@@ -371,46 +389,19 @@
             value = value + last[i].astype(f32)
         out_ref[:, cols(k)] = (mid_ref[:, cols(k)].astype(f32) + value).astype(bf16)
 
-    def run(steps):
-        for _, _, step, args in sorted(steps, key=lambda s: s[:2]):
-            step(*args)
-
-    meta_first()
-    for k in WIDE:
-        wide_first(k)
-    for k in range(CHUNKS):
-        own_tokens(k)
-    for h in range(1, 2):
-        meta_hop(h)
-    order = narrow + list(WIDE)
-    steps = []
-    for h in range(2, 5):
-        steps.append((h - 1, 0, meta_hop, (h,)))
-    steps.append((4, 4.5, tables, ()))
-    for t, k in enumerate(order):
-        for h in range(1, 5):
-            steps.append((t + h - 1, 5 - h, token_hop, (k, h)))
-        steps.append((t + 4, 5, select, (k,)))
-        if k not in WIDE:
-            steps.append((t + 5, 6, gather_rows, (k,)))
-            steps.append((t + 7, 7, forward_rows, (k,)))
-        steps.append((t + 9, 8, expert_in, (k, t == 0, t == CHUNKS - 1)))
-    run(steps)
-
-    order = list(WIDE) + narrow
-    steps = []
-    for t, k in enumerate(order):
-        steps.append((t, 5, expert_out, (k, t == 0)))
-        if k not in WIDE:
-            steps.append((t + 1, 6, reduce_hop, (k,)))
-            steps.append((t + 3, 7, reduce_rows, (k,)))
-        steps.append((t + 4, 8, combine, (k,)))
-        for h in range(1, 5):
-            steps.append((t + 4 + h, 5 - h, return_hop, (k, h)))
-        steps.append((t + 9, 0, finish, (k,)))
-        if k in WIDE:
-            steps.append((t + 11, 0.5, finish_wide, (k,)))
-    run(steps)
+    steps = (
+        meta_first, meta_hop, meta_wide_hop, tables, wide_first, token_hop, select, gather_rows, forward_rows,
+        expert_in, expert_out, reduce_hop, reduce_rows, combine, return_hop, finish, finish_wide,
+    )
+    done = {step: 0 for step in steps}
+    for number, *args in ORDER:
+        step = steps[number]
+        if step is expert_in:
+            args = args + [done[step] == 0, done[step] == CHUNKS - 1]
+        if step is expert_out:
+            args = args + [done[step] == 0]
+        done[step] += 1
+        step(*args)
     for name in net.copies:
         net.sent(name)
     assert net.used == sems.shape[0], net.used
@@ -449,7 +440,7 @@
 
     per_narrow = 7 + 7 + 6 + 6 + 7 + 7
     per_wide = 3 + 7 + 7 + 7 + 7 + 3
-    copies = 7 + (3 if WIDE else 0) + (CHUNKS - wides) * per_narrow + wides * per_wide
+    copies = 7 + (10 if WIDE else 0) + (CHUNKS - wides) * per_narrow + wides * per_wide
     any_spec = pl.BlockSpec(memory_space=pl.ANY)
     vmem_spec = pl.BlockSpec(memory_space=pltpu.VMEM)
     narrow_shapes, wide_shapes = group(CHUNKS - wides, 1), group(wides, NX)

time: 245 us -> 213 us (0.87)
  Pallas kernels: 206 us -> 174 us
    pallas_call x1, Pallas kernels: 206 us -> 174 us  [moe(): pl.pallas_call(body, out_shape=jax.ShapeDtypeStruct((toks, model), bf16),...]
  transfers between devices with their start and end apart: 5 -> 5, of which waited for: 1 -> 1; matrix products, arithmetic and copies ran while one was open for 2% -> 3% of each run, Pallas kernels for 0% -> 0%
where the time goes in v2:
time: 213 us; the launch traced here: 211 us
  Pallas kernels  174 us (82%)
  starting transfers between devices  15.4 us (7%)
  other arithmetic  7.36 us (3%)
  waiting for transfers between devices  5.31 us (2%)
  matrix products  4.5 us (2%)
  local copies, waits for them, and re-layouts  4.48 us (2%)
    pallas_call x1, Pallas kernels, moe(): pl.pallas_call(body, out_shape=jax.ShapeDtypeStruct((toks, model), bf16),...  174 us
    ppermute x2, starting transfers between devices, extended(): after = lax.ppermute(leading, axis, down)  7.28 us
    all_to_all x1, waiting for transfers between devices, per_device(): lax.all_to_all(att, 'tp', split_axis=0, concat_axis=1, tiled=True)  5.3 us
    all_to_all x1, starting transfers between devices, per_device(): lax.all_to_all(att, 'tp', split_axis=0, concat_axis=1, tiled=True)  4.29 us
  transfers between devices with their start and end apart: 5, of which 1 were waited for; matrix products, arithmetic and copies ran while one was open for 3% of the time, Pallas kernels for 0%

profile of v2, /device:TPU:8, one launch (start us, length us, event | category | flops | bytes accessed | tf_op | source)
XLA Modules:
  0.0 211.2 jit_solution(9296330111665560309)
XLA Ops:
  0.0 0.0 copy-start.2
  0.0 0.0 copy-start.6
  0.0 0.8 fusion.15
  0.8 0.8 fusion.17
  1.7 0.2 fusion.27
  1.9 0.8 pad_maximum_fusion.1
  2.6 1.9 collective-permute-start
  4.6 3.6 %collective-permute-start.1 = (bf16[128,128]{0,1:T(8,128)(2,1)S(1)}, bf16[128,128]{0,1:T(8,128)(2,1)S(1)}, u32[]{:S(2)}, u32[]{:S(2)}) collective-permute-start(bf16[128,128]{0,1:T(8,128)(2,1)S(1)} %get-tuple-element.10), channel_id=1, source_target_pairs={{4,0},{8,4},{12,8},{16,12},{20,16},{24,20},{28,24},{32,28},{36,32}... | collective-permute-start | bytes 98312 | tf_op jit(solution)/shard_map/ppermute | solution.py:49
  8.2 0.7 add_convert_fusion.2
  8.9 1.9 collective-permute-start.2
  10.8 3.6 %collective-permute-start.3 = (bf16[128]{0:T(256)(128)(2,1)S(1)}, bf16[128]{0:T(256)(128)(2,1)S(1)}, u32[]{:S(2)}, u32[]{:S(2)}) collective-permute-start(bf16[128]{0:T(256)(128)(2,1)S(1)} %get-tuple-element.14), channel_id=1, source_target_pairs={{4,0},{8,4},{12,8},{16,12},{20,16},{24,20},{28,24},{32,28},{36,32}... | collective-permute-start | bytes 776 | tf_op jit(solution)/shard_map/ppermute | solution.py:49
  14.5 0.2 multiply_cosine_fusion
  14.7 1.0 copy.23
  15.8 0.8 dynamic-slice_bitcast_fusion
  16.5 0.3 convert_reduce_fusion
  16.8 0.8 add_convert_fusion.1
  17.6 0.7 multiply_multiply_fusion
  18.4 0.0 copy-done.6
  18.4 0.0 collective-permute-done.2
  18.4 0.0 collective-permute-done.3
  18.4 0.2 fusion.7
  18.7 0.0 collective-permute-done
  18.7 0.0 collective-permute-done.1
  18.7 0.0 copy-done.2
  18.7 0.7 fusion.1
  19.4 0.1 broadcast_add_fusion
  19.4 0.0 copy-start.5
  19.5 0.6 fusion.2
  20.1 0.0 copy-start.1
  20.1 0.0 copy-start.4
  20.1 0.2 reshape.303
  20.3 0.8 copy.28
  21.1 4.3 %all-to-all-start = ((bf16[4,64,256]{2,1,0:T(8,128)(2,1)}), bf16[4,64,256]{2,1,0:T(8,128)(2,1)S(1)}, u32[]{:S(2)}, u32[]{:S(2)}) async-start(bf16[4,64,256]{2,1,0:T(8,128)(2,1)} %copy.28), calls=%async_computation | async-start | bytes 262144 | tf_op jit(solution)/shard_map/all_to_all | solution.py:560
  25.4 0.0 copy-done.5
  25.4 0.7 maximum_maximum_fusion.refs_1_
  26.1 5.3 %all-to-all-done = bf16[4,64,256]{2,1,0:T(8,128)(2,1)S(1)} async-done(((bf16[4,64,256]{2,1,0:T(8,128)(2,1)}), bf16[4,64,256]{2,1,0:T(8,128)(2,1)S(1)}, u32[]{:S(2)}, u32[]{:S(2)}) %all-to-all-start) | async-done | bytes 131104 | tf_op jit(solution)/shard_map/all_to_all | solution.py:560
  31.4 0.1 fusion.8
  31.5 0.0 copy-done.1
  31.6 0.0 copy-done.4
  31.6 0.0 copy-start.3
  31.6 3.2 %fusion.4 = (f32[64]{0:T(128)S(1)}, bf16[64,2048]{1,0:T(8,128)(2,1)S(1)}) fusion(bf16[1024,2048]{1,0:T(8,128)(2,1)} %param.25, f32[64,1024]{1,0:T(8,128)S(1)} %bitcast.49, f32[1024]{0:T(1024)S(1)} %copy-done.4, f32[64]{0:T(128)S(1)} %add_rsqrt_fusion.3, bf16[64,2048]{1,0:T(8,128)(2,1)S(1)} %copy-done.1), kind=kOutput, calls=%fused_computation.10 | convolution fusion | flops 269418432 | bytes 4985344 | tf_op jit(solution)/shard_map/dot_general | solution.py:563
  34.8 0.0 copy-start
  34.8 0.0 copy-done.3
  34.8 0.8 fusion.6.refs_0_
  35.7 0.0 copy-done
  35.7 173.9 %experts.1 = bf16[64,2048]{1,0:T(8,128)(2,1)} custom-call(bf16[64,2048]{1,0:T(8,128)(2,1)} %fusion.6.refs_0_, f32[16,128]{1,0:T(8,128)} %maximum_maximum_fusion.refs_1_, bf16[64,2048]{1,0:T(8,128)(2,1)} %copy-done, bf16[1,2048,512]{2,1,0:T(8,128)(2,1)} %refs_3_.1, bf16[1,2048,512]{2,1,0:T(8,128)(2,1)} %refs_4_.1, bf16[1,512,2048]{2,1,0:T(8,128)(2,1)} %refs_5_.1), custom_call_target="tpu_custom_call" | custom-call | tf_op jit(solution)/shard_map/experts/pallas_call | solution.py:458
  209.6 1.7 copy.31
  (18 shorter events, 0.2 us)
Async XLA Ops:
  0.0 18.7 %copy-start.2 = (bf16[256,64]{0,1:T(8,128)(2,1)S(1)}, bf16[256,64]{0,1:T(8,128)(2,1)}, u32[]{:S(2)}) copy-start(bf16[256,64]{0,1:T(8,128)(2,1)} %param.19) | copy-start | bytes 98308
  0.0 18.4 %copy-start.6 = (f32[4]{0:T(128)S(1)}, f32[4]{0:T(128)}, u32[]{:S(2)}) copy-start(f32[4]{0:T(128)} %param.23) | copy-start | bytes 52
  2.6 16.0 %collective-permute-start = (bf16[128,128]{0,1:T(8,128)(2,1)S(1)}, bf16[128,128]{0,1:T(8,128)(2,1)S(1)}, u32[]{:S(2)}, u32[]{:S(2)}) collective-permute-start(bf16[128,128]{0,1:T(8,128)(2,1)S(1)} %get-tuple-element.9), channel_id=1, source_target_pairs={{0,4},{4,8},{8,12},{12,16},{16,20},{20,24},{24,28},{28,32},{32,36}... | collective-permute-start | bytes 98312 | tf_op jit(solution)/shard_map/ppermute | solution.py:48
  4.6 14.1 %collective-permute-start.1 = (bf16[128,128]{0,1:T(8,128)(2,1)S(1)}, bf16[128,128]{0,1:T(8,128)(2,1)S(1)}, u32[]{:S(2)}, u32[]{:S(2)}) collective-permute-start(bf16[128,128]{0,1:T(8,128)(2,1)S(1)} %get-tuple-element.10), channel_id=1, source_target_pairs={{4,0},{8,4},{12,8},{16,12},{20,16},{24,20},{28,24},{32,28},{36,32}... | collective-permute-start | bytes 98312 | tf_op jit(solution)/shard_map/ppermute | solution.py:49
  8.9 9.5 %collective-permute-start.2 = (bf16[128]{0:T(256)(128)(2,1)S(1)}, bf16[128]{0:T(256)(128)(2,1)S(1)}, u32[]{:S(2)}, u32[]{:S(2)}) collective-permute-start(bf16[128]{0:T(256)(128)(2,1)S(1)} %get-tuple-element.13), channel_id=1, source_target_pairs={{0,4},{4,8},{8,12},{12,16},{16,20},{20,24},{24,28},{28,32},{32,36}... | collective-permute-start | bytes 776 | tf_op jit(solution)/shard_map/ppermute | solution.py:48
  10.8 7.6 %collective-permute-start.3 = (bf16[128]{0:T(256)(128)(2,1)S(1)}, bf16[128]{0:T(256)(128)(2,1)S(1)}, u32[]{:S(2)}, u32[]{:S(2)}) collective-permute-start(bf16[128]{0:T(256)(128)(2,1)S(1)} %get-tuple-element.14), channel_id=1, source_target_pairs={{4,0},{8,4},{12,8},{16,12},{20,16},{24,20},{28,24},{32,28},{36,32}... | collective-permute-start | bytes 776 | tf_op jit(solution)/shard_map/ppermute | solution.py:49
  19.4 5.9 %copy-start.5 = (f32[64,4]{0,1:T(4,128)S(1)}, f32[64,4]{0,1:T(4,128)}, u32[]{:S(2)}) copy-start(f32[64,4]{0,1:T(4,128)} %param.28) | copy-start | bytes 3076
  20.1 11.5 %copy-start.1 = (bf16[64,2048]{1,0:T(8,128)(2,1)S(1)}, bf16[64,2048]{1,0:T(8,128)(2,1)}, u32[]{:S(2)}) copy-start(bf16[64,2048]{1,0:T(8,128)(2,1)} %param.16) | copy-start | bytes 786436
  20.1 11.5 %copy-start.4 = (f32[1024]{0:T(1024)S(1)}, f32[1024]{0:T(1024)}, u32[]{:S(2)}) copy-start(f32[1024]{0:T(1024)} %param.24) | copy-start | bytes 12292
  21.1 10.3 %all-to-all-start = ((bf16[4,64,256]{2,1,0:T(8,128)(2,1)}), bf16[4,64,256]{2,1,0:T(8,128)(2,1)S(1)}, u32[]{:S(2)}, u32[]{:S(2)}) async-start(bf16[4,64,256]{2,1,0:T(8,128)(2,1)} %copy.28), calls=%async_computation | async-start | bytes 262144 | tf_op jit(solution)/shard_map/all_to_all | solution.py:560
  31.6 3.3 %copy-start.3 = (f32[2048]{0:T(1024)S(1)}, f32[2048]{0:T(1024)}, u32[]{:S(2)}) copy-start(f32[2048]{0:T(1024)} %param.26) | copy-start | bytes 24580
  34.8 0.9 copy-start

commit v3 on v2

--- a/solution.py
+++ b/solution.py
@@ -12,23 +12,24 @@
 PLANE = 8
 NX = 4
 CAP = 8
+HEAD = 64
 CHUNKS = 8
 WIDE = (6, 7)
-VMEM_LIMIT = 63 * 1024 * 1024
+VMEM_LIMIT = 67_043_328
 ORDER = (
-    (0,), (1, 1), (5, 1, 1), (5, 0, 1), (4, 6), (1, 2), (5, 1, 2), (5, 4, 1), (1, 3), (5, 1, 3), (5, 0, 2), (1, 4),
-    (5, 1, 4), (5, 4, 2), (4, 7), (5, 0, 3), (3, 0), (6, 1), (5, 3, 1), (5, 5, 1), (5, 2, 1), (5, 0, 4), (5, 4, 3),
-    (5, 3, 2), (5, 5, 2), (5, 2, 2), (7, 1), (5, 4, 4), (6, 0), (5, 7, 1), (5, 3, 3), (5, 2, 3), (8, 1), (6, 4),
-    (2, 1), (5, 5, 3), (7, 0), (5, 3, 4), (5, 7, 2), (6, 3), (2, 2), (7, 4), (5, 2, 4), (5, 5, 4), (8, 0),
-    (5, 7, 3), (8, 4), (6, 2), (6, 5), (2, 3), (5, 6, 1), (7, 3), (5, 7, 4), (2, 4), (7, 2), (5, 6, 2), (3, 1),
-    (6, 7), (5, 6, 3), (5, 6, 4), (7, 5), (9, 1), (8, 3), (9, 4), (6, 6), (9, 7), (8, 2), (8, 5), (9, 0), (9, 3),
-    (9, 2), (9, 5), (9, 6), (10, 6), (10, 7), (10, 0), (10, 1), (11, 1), (11, 0), (10, 2), (13, 6), (14, 6, 1),
-    (10, 3), (14, 6, 2), (12, 1), (13, 7), (12, 0), (14, 7, 1), (14, 6, 3), (14, 7, 2), (11, 2), (11, 3), (10, 4),
-    (12, 2), (13, 1), (14, 1, 1), (14, 7, 3), (14, 1, 2), (13, 0), (14, 6, 4), (11, 4), (14, 0, 1), (12, 3),
-    (10, 5), (13, 2), (14, 2, 1), (14, 1, 3), (14, 7, 4), (12, 4), (14, 1, 4), (14, 0, 2), (11, 5), (14, 2, 2),
-    (15, 7), (13, 3), (14, 3, 1), (15, 1), (14, 2, 3), (13, 4), (12, 5), (14, 4, 1), (14, 3, 2), (15, 6),
-    (14, 0, 3), (14, 3, 3), (14, 4, 2), (13, 5), (14, 5, 1), (14, 4, 3), (14, 5, 2), (14, 0, 4), (14, 5, 3),
-    (14, 4, 4), (14, 2, 4), (14, 3, 4), (15, 0), (14, 5, 4), (16, 6), (16, 7), (15, 4), (15, 3), (15, 2), (15, 5),
+    (0,), (1, 1), (5, 1, 1), (5, 0, 1), (4, 7), (1, 2), (4, 6), (5, 1, 2), (5, 3, 1), (1, 3), (5, 1, 3), (5, 0, 2),
+    (1, 4), (5, 1, 4), (5, 4, 1), (2, 1), (5, 0, 3), (3, 0), (5, 2, 1), (6, 1), (5, 4, 2), (5, 0, 4), (5, 5, 1),
+    (5, 3, 2), (5, 2, 2), (5, 4, 3), (7, 1), (5, 7, 1), (6, 0), (5, 4, 4), (8, 1), (5, 3, 3), (2, 2), (5, 3, 4),
+    (5, 5, 2), (7, 0), (5, 7, 2), (5, 2, 3), (6, 4), (2, 3), (6, 3), (8, 0), (5, 5, 3), (5, 2, 4), (7, 4),
+    (5, 7, 3), (5, 5, 4), (6, 2), (2, 4), (7, 3), (5, 6, 1), (5, 7, 4), (6, 5), (5, 6, 2), (8, 4), (7, 2), (3, 1),
+    (8, 3), (6, 7), (5, 6, 3), (9, 0), (8, 2), (5, 6, 4), (9, 4), (9, 1), (6, 6), (7, 5), (9, 2), (8, 5), (9, 7),
+    (9, 3), (9, 5), (9, 6), (10, 6), (10, 7), (10, 0), (10, 1), (11, 1), (11, 0), (10, 2), (10, 3), (13, 6),
+    (14, 6, 1), (12, 0), (14, 6, 2), (13, 7), (14, 7, 1), (12, 1), (13, 0), (14, 0, 1), (14, 7, 2), (11, 3),
+    (11, 2), (13, 1), (10, 4), (14, 6, 3), (12, 3), (14, 1, 1), (14, 7, 3), (12, 2), (11, 4), (14, 1, 2),
+    (14, 0, 2), (14, 6, 4), (10, 5), (14, 7, 4), (13, 2), (14, 2, 1), (12, 4), (13, 3), (14, 3, 1), (14, 1, 3),
+    (11, 5), (14, 0, 3), (14, 2, 2), (15, 6), (13, 4), (14, 4, 1), (14, 1, 4), (12, 5), (14, 3, 2), (14, 0, 4),
+    (15, 7), (14, 4, 2), (14, 2, 3), (13, 5), (14, 5, 1), (16, 6), (14, 4, 3), (14, 5, 2), (14, 3, 3), (14, 5, 3),
+    (14, 4, 4), (14, 2, 4), (15, 1), (15, 0), (14, 3, 4), (14, 5, 4), (15, 4), (15, 3), (16, 7), (15, 2), (15, 5),
 )
 
 
@@ -36,39 +37,6 @@
 norm_eps = 1e-06
 swiglu_limit = 7.0
 swiglu_alpha = 1.702
-
-
-def extended(x, sides, width):
-    for axis, dim in sides:
-        peers, length = (lax.axis_size(axis), x.shape[dim])
-        up = [(i, (i + 1) % peers) for i in range(peers - 1)]
-        down = [(j, i) for i, j in up]
-        last = lax.slice_in_dim(x, length - width, length, axis=dim)
-        leading = lax.slice_in_dim(x, 0, width, axis=dim)
-        before = lax.ppermute(last, axis, up)
-        after = lax.ppermute(leading, axis, down)
-        x = jnp.concatenate([before, x, after], axis=dim)
-    return x
-
-
-def row_normalize(values, gain_vec):
-    floats = values.astype(jnp.float32)
-    scale_inv = lax.rsqrt(jnp.mean(floats * floats, axis=-1, keepdims=True) + norm_eps)
-    return floats * scale_inv * gain_vec
-
-
-def apply_rotary_heads(heads, token_positions):
-    half_size = heads.shape[-1] // 2
-    freqs = rope_base ** (-jnp.arange(half_size, dtype=jnp.float32) / half_size)
-    angles = token_positions[:, None] * freqs[None, :]
-    cosine = jnp.cos(angles)[:, None, :]
-    sine = jnp.sin(angles)[:, None, :]
-    first_half = heads[..., :half_size]
-    second_half = heads[..., half_size:]
-    return jnp.concatenate(
-        [first_half * cosine - second_half * sine, first_half * sine + second_half * cosine],
-        axis=-1,
-    )
 
 
 class Net:
@@ -100,13 +68,15 @@
 
 
 def moe_kernel(
-    tok_ref, meta_ref, mid_ref, wg_hbm, wu_hbm, wd_hbm, out_ref,
+    q_ref, kv_ref, doc_ref, angle_ref, gain_ref, sink_ref, out_gain_ref, norm_gain_ref, resid_ref, meta_ref,
+    wo_hbm, wg_hbm, wu_hbm, wd_hbm, out_ref,
+    wo, q_rot, kv_span, doc_span, att, by_token, mid_ref,
     wg, wu, wd, rows, gate_acc, up_acc, hidden, meta, pick, mix_hi, mix_lo,
     scr_narrow, scr_wide, sems, wsem,
 ):
     bf16, f32 = jnp.bfloat16, jnp.float32
-    width = tok_ref.shape[1] // CHUNKS
-    toks = tok_ref.shape[0]
+    toks, model = resid_ref.shape
+    width = model // CHUNKS
     block = PLANE * toks
     half = block // 2
     sp, x = lax.axis_index("sp"), lax.axis_index("tp")
@@ -133,19 +103,109 @@
         pltpu.make_async_copy(src.at[0], dst, wsem.at[i])
         for i, (src, dst) in enumerate(((wg_hbm, wg), (wu_hbm, wu), (wd_hbm, wd)))
     ]
+    project_copy = pltpu.make_async_copy(wo_hbm, wo, wsem.at[3])
+    project_copy.start()
     for copy in weight_copies:
         copy.start()
 
     meta[0, 0] = meta_ref[...]
-    for k in range(CHUNKS):
-        buf(k, "spread")[0, 0] = tok_ref[:, cols(k)]
+    held = kv_ref.shape[0]
+    lanes = 2 * HEAD
+
+    def head_mean(squares):
+        r = lax.broadcasted_iota(jnp.int32, (lanes, lanes), 0) // HEAD
+        c = lax.broadcasted_iota(jnp.int32, (lanes, lanes), 1) // HEAD
+        spread_out = jnp.where(r == c, 1.0 / HEAD, 0.0).astype(f32)
+        return jnp.dot(squares, spread_out, preferred_element_type=f32, precision=lax.Precision.HIGHEST)
+
+    def normed_rotated(value, gain):
+        scaled = value * lax.rsqrt(head_mean(value * value) + norm_eps) * gain
+        lane = lax.broadcasted_iota(jnp.int32, value.shape, 1)
+        first = lax.rem(lane, HEAD) < HEAD // 2
+        turned = jnp.where(
+            first, -pltpu.roll(scaled, lanes - HEAD // 2, axis=1), pltpu.roll(scaled, HEAD // 2, axis=1)
+        )
+        return scaled * angle_ref[:, :lanes] + turned * angle_ref[:, lanes:]
+
+    own = pl.ds(WINDOW, held)
+    kv = kv_ref[...].astype(f32)
+    on_key = lax.broadcasted_iota(jnp.int32, kv.shape, 1) < HEAD
+    kv_span[own, :] = jnp.where(on_key, normed_rotated(kv, gain_ref[1:2, :]), kv).astype(bf16)
+    doc_span[:, own] = doc_ref[...]
 
     barrier = pltpu.get_barrier_semaphore()
-    peers = [up, down, right, left] + ahead[1:] + ([far] if WIDE else [])
+    count = NZ * PLANE
+    after, before = (lax.rem(sp + 1, count), x), (lax.rem(sp + count - 1, count), x)
+    peers = [up, down, right, left, after, before, far] + ahead[1:]
     for peer in peers:
         pl.semaphore_signal(barrier, inc=1, device_id=peer, device_id_type=MESH)
     pl.semaphore_wait(barrier, len(peers))
 
+    low_rows, high_rows = pl.ds(0, WINDOW), pl.ds(held + WINDOW, WINDOW)
+    net.send("kv+", kv_span.at[pl.ds(held, WINDOW), :], kv_span.at[low_rows, :], after)
+    net.send("kv-", kv_span.at[pl.ds(WINDOW, WINDOW), :], kv_span.at[high_rows, :], before)
+    net.send("doc+", doc_ref.at[:, pl.ds(held - WINDOW, WINDOW)], doc_span.at[:, low_rows], after)
+    net.send("doc-", doc_ref.at[:, pl.ds(0, WINDOW)], doc_span.at[:, high_rows], before)
+    pairs = q_ref.shape[1] // lanes
+    for i in range(pairs):
+        part = slice(i * lanes, (i + 1) * lanes)
+        q_rot[:, part] = normed_rotated(q_ref[:, part].astype(f32), gain_ref[0:1, :]).astype(bf16)
+    for name in ("kv+", "kv-", "doc+", "doc-"):
+        net.arrived(name)
+    both = kv_span[...].astype(f32)
+    swapped = pltpu.roll(both, HEAD, axis=1)
+    on_key = lax.broadcasted_iota(jnp.int32, both.shape, 1) < HEAD
+    key_twice = jnp.where(on_key, both, swapped).astype(bf16)
+    value_twice = jnp.where(on_key, swapped, both).astype(bf16)
+    span = held + 2 * WINDOW
+    query_at = lax.broadcasted_iota(jnp.int32, (held, span), 0)
+    key_at = lax.broadcasted_iota(jnp.int32, (held, span), 1) - WINDOW
+    place_at = sp * held + key_at
+    allowed = (jnp.abs(query_at - key_at) <= WINDOW) & (place_at >= 0) & (place_at < count * held)
+    allowed = allowed & (doc_ref[...].T[:, 0:1] == doc_span[0:1, :])
+    in_first = lax.broadcasted_iota(jnp.int32, (held, lanes), 1) < HEAD
+    for i in range(pairs):
+        mixed_pair = []
+        for j in range(2):
+            q = q_rot[:, i * lanes : (i + 1) * lanes]
+            q = jnp.where(in_first if j == 0 else ~in_first, q.astype(f32), 0.0).astype(bf16)
+            scores = lax.dot_general(q, key_twice, (((1,), (1,)), ((), ())), preferred_element_type=f32)
+            raw = jnp.where(allowed, jnp.exp(scores * HEAD ** (-0.5)), 0.0)
+            h = 2 * i + j
+            total = jnp.sum(raw, axis=1, keepdims=True) + jnp.exp(sink_ref[0:1, h : h + 1])
+            mixed_pair.append(jnp.dot((raw / total).astype(bf16), value_twice, preferred_element_type=f32))
+        att[:, i * lanes : (i + 1) * lanes] = jnp.where(in_first, mixed_pair[0], mixed_pair[1]).astype(bf16)
+    for d, peer in ((2, far), (1, right), (3, left)):
+        other = pl.multiple_of(lax.rem(x + d, NX) * toks, toks)
+        net.send(("att", d), att.at[pl.ds(other, toks), :], by_token.at[x], peer)
+    by_token[x] = att[pl.ds(pl.multiple_of(x * toks, toks), toks), :]
+    project_copy.wait()
+    for d in (1, 2, 3):
+        net.arrived(("att", d))
+    channels = att.shape[1]
+    pieces = [by_token[i].astype(f32) for i in range(NX)]
+    square = sum(jnp.sum(piece * piece, axis=1, keepdims=True) for piece in pieces)
+    inverse = lax.rsqrt(square / (NX * channels) + norm_eps)
+    pieces = [
+        (piece * inverse * out_gain_ref[0:1, i * channels : (i + 1) * channels]).astype(bf16)
+        for i, piece in enumerate(pieces)
+    ]
+    for k in range(CHUNKS):
+        made = resid_ref[:, cols(k)].astype(f32)
+        made = made + sum(
+            jnp.dot(piece, wo[i * channels : (i + 1) * channels, cols(k)], preferred_element_type=f32)
+            for i, piece in enumerate(pieces)
+        )
+        mid_ref[:, cols(k)] = made.astype(bf16)
+    square = jnp.zeros((toks, 1), f32)
+    for k in range(CHUNKS):
+        value = mid_ref[:, cols(k)].astype(f32)
+        square = square + jnp.sum(value * value, axis=1, keepdims=True)
+    inverse = lax.rsqrt(square / model + norm_eps)
+    for k in range(CHUNKS):
+        value = mid_ref[:, cols(k)].astype(f32) * inverse * norm_gain_ref[0:1, cols(k)]
+        buf(k, "spread")[0, 0] = value.astype(bf16)
+
     meta_width = NX if WIDE else 1
 
     def up_hops(k):
@@ -159,7 +219,7 @@
 
     def wide_first(k):
         spread = buf(k, "spread")
-        src = tok_ref.at[:, cols(k)]
+        src = spread.at[0, 0]
         net.send((k, "w", 1), src, spread.at[0, 1], right)
         net.send((k, "w", 2), src, spread.at[0, 2], left)
         net.send((k, "w", 3), src, spread.at[0, 3], far)
@@ -232,10 +292,10 @@
                 got = jnp.dot(pick[xi, i], pair, preferred_element_type=f32).astype(bf16)
                 rows[k, xi, 16 * i : 16 * i + 16, :] = got[0:16]
                 for q in range(1, PLANE):
-                    chosen[q, xi, 16 * i : 16 * i + 16, :] = got[16 * q : 16 * q + 16]
+                    chosen[q - 1, xi, 16 * i : 16 * i + 16, :] = got[16 * q : 16 * q + 16]
         for q in (4, 5, 2, 3, 6, 7, 1):
             net.send(
-                (k, "y", q), chosen.at[q],
+                (k, "y", q), chosen.at[q - 1],
                 rows.at[k, pl.ds(0, place[k][2]), pl.ds(q * toks, toks), :], ahead[q],
             )
 
@@ -309,7 +369,7 @@
         if k in WIDE:
             back = buf(k, "back")
             for q in (4, 5, 2, 3, 6, 7, 1):
-                net.send((k, "b", q), rows.at[k, pl.ds(0, NX), pl.ds(q * toks, toks), :], back.at[q], behind[q])
+                net.send((k, "b", q), rows.at[k, pl.ds(0, NX), pl.ds(q * toks, toks), :], back.at[q - 1], behind[q])
         else:
             net.send((k, "oA"), rows.at[k, 3, a, :], buf(k, "hop_r"), right)
             net.send((k, "oB"), rows.at[k, 3, b, :], buf(k, "hop_l"), left)
@@ -333,7 +393,7 @@
             rows[k, 0].astype(f32) + buf(k, "sum_r")[...].astype(f32) + buf(k, "sum_l")[...].astype(f32)
         ).astype(bf16)
         for q in (4, 5, 2, 3, 6, 7, 1):
-            net.send((k, "b", q), total.at[pl.ds(q * toks, toks), :], back.at[q, 0], behind[q])
+            net.send((k, "b", q), total.at[pl.ds(q * toks, toks), :], back.at[q - 1, 0], behind[q])
 
     def combine(k):
         for q in range(1, PLANE):
@@ -343,7 +403,7 @@
             for i in range(NZ // 2):
                 part = slice(16 * i, 16 * i + 16)
                 own = rows[k, xi, part, :] if k in WIDE else buf(k, "total")[part, :]
-                outs = jnp.concatenate([own] + [back[q, xi, part, :] for q in range(1, PLANE)], axis=0)
+                outs = jnp.concatenate([own] + [back[q - 1, xi, part, :] for q in range(1, PLANE)], axis=0)
                 got = jnp.dot(mix_hi[xi, i], outs, preferred_element_type=f32)
                 got = got + jnp.dot(mix_lo[xi, i], outs, preferred_element_type=f32)
                 mixed[2 * i, xi] = got[:toks]
@@ -407,9 +467,10 @@
     assert net.used == sems.shape[0], net.used
 
 
-def moe(tokens, meta, middle, w_gate, w_up, w_down):
+def layer(queries, key_value, doc_rows, angles, gains, sink, out_gain, norm_gain, resid, meta, w_out, w_gate, w_up, w_down):
     bf16, f32 = jnp.bfloat16, jnp.float32
-    toks, model = tokens.shape
+    toks, model = resid.shape
+    held, channels = queries.shape
     width = model // CHUNKS
     units = w_gate.shape[2]
     block = PLANE * toks
@@ -421,8 +482,8 @@
             return {"none": pltpu.VMEM((16, 128), bf16)}
         shapes = {
             "spread": pltpu.VMEM((count, NZ, nx, toks, width), bf16),
-            "chosen": pltpu.VMEM((count, PLANE, nx, toks, width), bf16),
-            "back": pltpu.VMEM((count, PLANE, nx, toks, width), bf16),
+            "chosen": pltpu.VMEM((count, PLANE - 1, nx, toks, width), bf16),
+            "back": pltpu.VMEM((count, PLANE - 1, nx, toks, width), bf16),
             "mixed": pltpu.VMEM((count, NZ, nx, toks, width), f32),
             "leaving": pltpu.VMEM((count, NZ, nx, toks, width), bf16),
             "from_up": pltpu.VMEM((count, 4, nx, toks, width), bf16),
@@ -440,14 +501,14 @@
 
     per_narrow = 7 + 7 + 6 + 6 + 7 + 7
     per_wide = 3 + 7 + 7 + 7 + 7 + 3
-    copies = 7 + (10 if WIDE else 0) + (CHUNKS - wides) * per_narrow + wides * per_wide
+    copies = 7 + 7 + (10 if WIDE else 0) + (CHUNKS - wides) * per_narrow + wides * per_wide
     any_spec = pl.BlockSpec(memory_space=pl.ANY)
     vmem_spec = pl.BlockSpec(memory_space=pltpu.VMEM)
     narrow_shapes, wide_shapes = group(CHUNKS - wides, 1), group(wides, NX)
     names_n, names_w = list(narrow_shapes), list(wide_shapes)
 
     def body(*refs):
-        fixed, rest = refs[:18], refs[18:]
+        fixed, rest = refs[:33], refs[33:]
         scr_n = dict(zip(names_n, rest[: len(names_n)]))
         rest = rest[len(names_n) :]
         scr_w = dict(zip(names_w, rest[: len(names_w)]))
@@ -458,9 +519,16 @@
     return pl.pallas_call(
         body,
         out_shape=jax.ShapeDtypeStruct((toks, model), bf16),
-        in_specs=[vmem_spec, vmem_spec, vmem_spec, any_spec, any_spec, any_spec],
+        in_specs=[vmem_spec] * 10 + [any_spec] * 4,
         out_specs=vmem_spec,
         scratch_shapes=[
+            pltpu.VMEM(w_out.shape, bf16),
+            pltpu.VMEM((held, channels), bf16),
+            pltpu.VMEM((held + 2 * WINDOW, 2 * HEAD), bf16),
+            pltpu.VMEM((8, held + 2 * WINDOW), f32),
+            pltpu.VMEM((held, channels), bf16),
+            pltpu.VMEM((NX, toks, channels), bf16),
+            pltpu.VMEM((toks, model), bf16),
             pltpu.VMEM((model, units), bf16),
             pltpu.VMEM((model, units), bf16),
             pltpu.VMEM((units, model), bf16),
@@ -473,13 +541,13 @@
             *narrow_shapes.values(),
             *wide_shapes.values(),
             pltpu.SemaphoreType.DMA((2 * copies,)),
-            pltpu.SemaphoreType.DMA((3,)),
+            pltpu.SemaphoreType.DMA((4,)),
         ],
         compiler_params=pltpu.CompilerParams(
             collective_id=0, has_side_effects=True, vmem_limit_bytes=VMEM_LIMIT
         ),
-        name="experts",
-    )(tokens, meta, middle, w_gate, w_up, w_down)
+        name="layer",
+    )(queries, key_value, doc_rows, angles, gains, sink, out_gain, norm_gain, resid, meta, w_out, w_gate, w_up, w_down)
 
 
 def route_table(own_routes, weights):
@@ -516,57 +584,32 @@
     tp_size = lax.axis_size("tp")
     sp_index = lax.axis_index("sp")
     tp_index = lax.axis_index("tp")
-    tok_rows = queries.shape[0]
-    head_size = q_gain.shape[0]
-    query_heads = sink.shape[0]
-    kv_heads = keys.shape[1] // head_size
-    query_group_width = query_heads // kv_heads
-    token_positions = (sp_index * tok_rows + jnp.arange(tok_rows, dtype=jnp.int32)).astype(
-        jnp.float32
+    f32 = jnp.float32
+    held = queries.shape[0]
+    positions = (sp_index * held + jnp.arange(held, dtype=jnp.int32)).astype(f32)
+    half = HEAD // 2
+    freqs = rope_base ** (-jnp.arange(half, dtype=f32) / half)
+    turns = positions[:, None] * jnp.tile(freqs, 2 * HEAD // half)[None, :]
+    angles = jnp.concatenate([jnp.cos(turns), jnp.sin(turns)], axis=1)
+    gains = jnp.stack([jnp.tile(q_gain, 2), jnp.tile(key_norm_gain, 2)])
+    quarter = held // lax.axis_size("tp")
+    own_routes = lax.dynamic_slice_in_dim(routes, tp_index * quarter, quarter, 0)
+    return layer(
+        queries,
+        jnp.concatenate([keys, values], axis=1),
+        jnp.broadcast_to(docs.astype(f32)[None, :], (8, held)),
+        angles,
+        gains,
+        sink[None, :],
+        out_gain[None, :],
+        norm_gain[None, :],
+        resid,
+        route_table(own_routes, route_weights),
+        w_out,
+        w_gate,
+        w_up,
+        w_down,
     )
-    q_rot = apply_rotary_heads(
-        row_normalize(queries.reshape(tok_rows, query_heads, head_size), q_gain), token_positions
-    ).astype(jnp.bfloat16)
-    key_rotated = apply_rotary_heads(
-        row_normalize(keys.reshape(tok_rows, kv_heads, head_size), key_norm_gain), token_positions
-    ).astype(jnp.bfloat16)
-    key_value = jnp.concatenate(
-        [key_rotated.reshape(tok_rows, kv_heads * head_size), values], axis=1
-    )
-    doc_mark = (docs + 1).astype(jnp.bfloat16)
-    kv_span, doc_span = (
-        extended(key_value, (("sp", 0),), WINDOW),
-        extended(doc_mark, (("sp", 0),), WINDOW),
-    )
-    span_rows = tok_rows + 2 * WINDOW
-    k_span = kv_span[:, : kv_heads * head_size].reshape(span_rows, kv_heads, head_size)
-    v_span = kv_span[:, kv_heads * head_size :].reshape(span_rows, kv_heads, head_size)
-    scores = jnp.einsum(
-        "qhgd,khd->hgqk",
-        q_rot.reshape(tok_rows, kv_heads, query_group_width, head_size),
-        k_span,
-        preferred_element_type=jnp.float32,
-    ) * head_size ** (-0.5)
-    offsets = jnp.arange(tok_rows, dtype=jnp.int32)[:, None] - (
-        jnp.arange(span_rows, dtype=jnp.int32)[None, :] - WINDOW
-    )
-    allowed = (jnp.abs(offsets) <= WINDOW) & (doc_mark[:, None] == doc_span[None, :])
-    raw_weights = jnp.where(allowed[None, None], jnp.exp(scores), jnp.zeros((), jnp.float32))
-    sink_exponent = jnp.exp(sink).reshape(kv_heads, query_group_width)
-    total = jnp.sum(raw_weights, axis=-1) + sink_exponent[:, :, None]
-    probs = (raw_weights / total[..., None]).astype(jnp.bfloat16)
-    att = jnp.einsum("hgqk,khd->qhgd", probs, v_span, preferred_element_type=jnp.float32)
-    att = att.astype(jnp.bfloat16).reshape(tok_rows, query_heads * head_size)
-    by_token = lax.all_to_all(att, "tp", split_axis=0, concat_axis=1, tiled=True)
-    att_normed = row_normalize(by_token, out_gain).astype(jnp.bfloat16)
-    middle = (
-        resid.astype(jnp.float32) + jnp.dot(att_normed, w_out, preferred_element_type=jnp.float32)
-    ).astype(jnp.bfloat16)
-    moe_in = row_normalize(middle, norm_gain).astype(jnp.bfloat16)
-    quarter = tok_rows // tp_size
-    own_routes = lax.dynamic_slice_in_dim(routes, tp_index * quarter, quarter, 0)
-    table = route_table(own_routes, route_weights)
-    return moe(moe_in, table, middle, w_gate, w_up, w_down)
 
 
 def solution(mesh):

time: 213 us -> 193 us (0.906)
  starting transfers between devices: 15.4 us -> 0 us
  Pallas kernels: 174 us -> 181 us
  waiting for transfers between devices: 5.31 us -> 0 us
  matrix products: 4.5 us -> 0 us
    ppermute x4 -> x0, starting transfers between devices: 11.1 us -> none  [the longest x2 7.28 us: extended(): after = lax.ppermute(leading, axis, down)]
    pallas_call x1, Pallas kernels: 174 us -> 181 us  [layer(): pl.pallas_call(body, out_shape=jax.ShapeDtypeStruct((toks, model), bf16),...]
    all_to_all x1 -> x0, waiting for transfers between devices: 5.3 us -> none  [per_device(): lax.all_to_all(att, 'tp', split_axis=0, concat_axis=1, tiled=True)]
    dot_general x3 -> x0, matrix products: 4.5 us -> none  [the longest x1 3.21 us: per_device(): jnp.dot(att_normed, w_out, preferred_element_type=jnp.float32)]
    all_to_all x1 -> x0, starting transfers between devices: 4.29 us -> none  [per_device(): lax.all_to_all(att, 'tp', split_axis=0, concat_axis=1, tiled=True)]
  transfers between devices with their start and end apart: 5 -> 0, of which waited for: 1 -> 0; matrix products, arithmetic and copies ran while one was open for 3% -> 0% of each run, Pallas kernels for 0% -> 0%
where the time goes in v3:
time: 193 us
  Pallas kernels  181 us (94%)
  local copies, waits for them, and re-layouts  6.33 us (3%)
  other arithmetic  5.68 us (3%)
    pallas_call x1, Pallas kernels, layer(): pl.pallas_call(body, out_shape=jax.ShapeDtypeStruct((toks, model), bf16),...  181 us

profile of v3, /device:TPU:8, one launch (start us, length us, event | category | flops | bytes accessed | tf_op | source)
XLA Modules:
  0.0 192.8 jit_solution(15330111756013348474)
XLA Ops:
  0.0 0.7 convert_element_type.16
  0.7 0.7 tile.7
  1.4 0.1 stack_tile.6
  1.4 0.7 tile.8
  2.1 0.1 stack_tile.7
  2.2 0.5 pad_maximum_fusion.2.refs_4_
  2.7 0.1 mul.29
  2.8 0.8 dynamic-slice_bitcast_fusion
  3.6 0.6 broadcast_in_dim.10.refs_2_
  4.2 0.3 convert_reduce_fusion
  4.4 0.8 add_convert_fusion
  5.2 1.4 maximum_maximum_fusion.refs_9_
  6.6 0.9 copy.19
  7.5 0.9 copy.20
  8.4 0.7 pad_maximum_fusion.1.refs_1_
  9.1 0.5 multiply_cosine_fusion
  9.6 0.7 pad_maximum_fusion.refs_3_
  10.4 180.7 %layer.1 = bf16[64,2048]{1,0:T(8,128)(2,1)} custom-call(bf16[256,256]{1,0:T(8,128)(2,1)} %refs_0_.1, bf16[256,128]{1,0:T(8,128)(2,1)} %pad_maximum_fusion.1.refs_1_, f32[8,256]{1,0:T(8,128)} %broadcast_in_dim.10.refs_2_, f32[256,256]{1,0:T(8,128)} %pad_maximum_fusion.refs_3_, f32[2,128]{1,0:T(2,128)} %pad_maximum_fusion.2.refs_4_, f32[1,4]{1,0:T(1,128)} %bitcast.11, ...), custom_call_target="tpu_custom_call" | custom-call | tf_op jit(solution)/shard_map/layer/pallas_call | solution.py:519
  191.1 1.7 copy.22
  (5 shorter events, 0.0 us)

commit v4 on v3

--- a/solution.py
+++ b/solution.py
@@ -44,31 +44,57 @@
         self.sems = sems
         self.used = 0
         self.copies = {}
-
-    def send(self, name, src, dst, device):
+        self.groups = {}
+
+    def semaphore(self):
+        self.used += 1
+        return self.sems.at[self.used - 1]
+
+    def group(self, kind, key, whole, device):
+        if (kind, key) not in self.groups:
+            sem = self.semaphore()
+            copy = pltpu.make_async_remote_copy(
+                src_ref=whole, dst_ref=whole, send_sem=sem, recv_sem=sem, device_id=device, device_id_type=MESH
+            )
+            self.groups[kind, key] = [sem, copy, False]
+        return self.groups[kind, key][0]
+
+    def send(self, name, src, dst, device, out=None, into=None):
         copy = pltpu.make_async_remote_copy(
             src_ref=src,
             dst_ref=dst,
-            send_sem=self.sems.at[self.used],
-            recv_sem=self.sems.at[self.used + 1],
+            send_sem=self.group("out", *out, device) if out else self.semaphore(),
+            recv_sem=self.group("into", *into, device) if into else self.semaphore(),
             device_id=device,
             device_id_type=MESH,
         )
-        self.used += 2
         copy.start()
-        self.copies[name] = [copy, False]
+        self.copies[name] = (copy, out is None)
 
     def arrived(self, name):
         self.copies[name][0].wait_recv()
 
-    def sent(self, name):
-        if not self.copies[name][1]:
-            self.copies[name][0].wait_send()
-            self.copies[name][1] = True
+    def all_arrived(self, key):
+        self.groups["into", key][1].wait_recv()
+
+    def all_sent(self, key):
+        group = self.groups["out", key]
+        if not group[2]:
+            group[1].wait_send()
+            group[2] = True
+
+    def finish(self):
+        for kind, key in self.groups:
+            if kind == "out":
+                self.all_sent(key)
+        for copy, alone in self.copies.values():
+            if alone:
+                copy.wait_send()
 
 
 def moe_kernel(
-    q_ref, kv_ref, doc_ref, angle_ref, gain_ref, sink_ref, out_gain_ref, norm_gain_ref, resid_ref, meta_ref,
+    q_ref, key_ref, value_ref, doc_ref, cos_ref, sin_ref, q_gain_ref, k_gain_ref, sink_ref, out_gain_ref,
+    norm_gain_ref, resid_ref, slot_ref, weight_ref,
     wo_hbm, wg_hbm, wu_hbm, wd_hbm, out_ref,
     wo, q_rot, kv_span, doc_span, att, by_token, mid_ref,
     wg, wu, wd, rows, gate_acc, up_acc, hidden, meta, pick, mix_hi, mix_lo,
@@ -108,8 +134,10 @@
     for copy in weight_copies:
         copy.start()
 
-    meta[0, 0] = meta_ref[...]
-    held = kv_ref.shape[0]
+    held = q_ref.shape[0]
+    table = jnp.concatenate([slot_ref[...], weight_ref[...]], axis=0)
+    table = jnp.concatenate([table, table], axis=1)
+    meta[0, 0] = jnp.concatenate([table, table], axis=0)
     lanes = 2 * HEAD
 
     def head_mean(squares):
@@ -125,13 +153,15 @@
         turned = jnp.where(
             first, -pltpu.roll(scaled, lanes - HEAD // 2, axis=1), pltpu.roll(scaled, HEAD // 2, axis=1)
         )
-        return scaled * angle_ref[:, :lanes] + turned * angle_ref[:, lanes:]
+        return scaled * cos_ref[...] + turned * sin_ref[...]
 
     own = pl.ds(WINDOW, held)
-    kv = kv_ref[...].astype(f32)
+    kv = jnp.concatenate([key_ref[...], value_ref[...]], axis=0).astype(f32).T
+    q_gain = jnp.concatenate([q_gain_ref[...], q_gain_ref[...]], axis=1)
+    k_gain = jnp.concatenate([k_gain_ref[...], k_gain_ref[...]], axis=1)
     on_key = lax.broadcasted_iota(jnp.int32, kv.shape, 1) < HEAD
-    kv_span[own, :] = jnp.where(on_key, normed_rotated(kv, gain_ref[1:2, :]), kv).astype(bf16)
-    doc_span[:, own] = doc_ref[...]
+    kv_span[own, :] = jnp.where(on_key, normed_rotated(kv, k_gain), kv).astype(bf16)
+    doc_span[:, own] = jnp.broadcast_to(doc_ref[...].astype(f32), (8, held))
 
     barrier = pltpu.get_barrier_semaphore()
     count = NZ * PLANE
@@ -144,12 +174,12 @@
     low_rows, high_rows = pl.ds(0, WINDOW), pl.ds(held + WINDOW, WINDOW)
     net.send("kv+", kv_span.at[pl.ds(held, WINDOW), :], kv_span.at[low_rows, :], after)
     net.send("kv-", kv_span.at[pl.ds(WINDOW, WINDOW), :], kv_span.at[high_rows, :], before)
-    net.send("doc+", doc_ref.at[:, pl.ds(held - WINDOW, WINDOW)], doc_span.at[:, low_rows], after)
-    net.send("doc-", doc_ref.at[:, pl.ds(0, WINDOW)], doc_span.at[:, high_rows], before)
+    net.send("doc+", doc_span.at[:, pl.ds(held, WINDOW)], doc_span.at[:, low_rows], after)
+    net.send("doc-", doc_span.at[:, pl.ds(WINDOW, WINDOW)], doc_span.at[:, high_rows], before)
     pairs = q_ref.shape[1] // lanes
     for i in range(pairs):
         part = slice(i * lanes, (i + 1) * lanes)
-        q_rot[:, part] = normed_rotated(q_ref[:, part].astype(f32), gain_ref[0:1, :]).astype(bf16)
+        q_rot[:, part] = normed_rotated(q_ref[:, part].astype(f32), q_gain).astype(bf16)
     for name in ("kv+", "kv-", "doc+", "doc-"):
         net.arrived(name)
     both = kv_span[...].astype(f32)
@@ -162,7 +192,7 @@
     key_at = lax.broadcasted_iota(jnp.int32, (held, span), 1) - WINDOW
     place_at = sp * held + key_at
     allowed = (jnp.abs(query_at - key_at) <= WINDOW) & (place_at >= 0) & (place_at < count * held)
-    allowed = allowed & (doc_ref[...].T[:, 0:1] == doc_span[0:1, :])
+    allowed = allowed & (doc_span[:, own].T[:, 0:1] == doc_span[0:1, :])
     in_first = lax.broadcasted_iota(jnp.int32, (held, lanes), 1) < HEAD
     for i in range(pairs):
         mixed_pair = []
@@ -220,25 +250,27 @@
     def wide_first(k):
         spread = buf(k, "spread")
         src = spread.at[0, 0]
-        net.send((k, "w", 1), src, spread.at[0, 1], right)
-        net.send((k, "w", 2), src, spread.at[0, 2], left)
-        net.send((k, "w", 3), src, spread.at[0, 3], far)
+        out = ((k, "w"), spread.at[0, pl.ds(1, 3)])
+        net.send((k, "w", 1), src, spread.at[0, 1], right, out)
+        net.send((k, "w", 2), src, spread.at[0, 2], left, out)
+        net.send((k, "w", 3), src, spread.at[0, 3], far, out)
 
     def meta_first():
         if WIDE:
-            net.send(("mw", 1), meta_ref, meta.at[0, 1], right)
-            net.send(("mw", 2), meta_ref, meta.at[0, 2], left)
-            net.send(("mw", 3), meta_ref, meta.at[0, 3], far)
+            net.send(("mw", 1), meta.at[0, 0], meta.at[0, 1], right, ("mw", meta.at[0, pl.ds(1, 3)]))
+            net.send(("mw", 2), meta.at[0, 0], meta.at[0, 2], left, ("mw", meta.at[0, pl.ds(1, 3)]))
+            net.send(("mw", 3), meta.at[0, 0], meta.at[0, 3], far, ("mw", meta.at[0, pl.ds(1, 3)]))
 
     def ring_hop(name, h, last_up, last_down, data):
+        out = ((name, "z"), data.at[pl.ds(1, NZ - 1)])
         if h <= last_up:
             if h > 1:
                 net.arrived((name, "u", h - 1))
-            net.send((name, "u", h), data.at[up_slot(h - 1)], data.at[up_slot(h)], up)
+            net.send((name, "u", h), data.at[up_slot(h - 1)], data.at[up_slot(h)], up, out)
         if h <= last_down:
             if h > 1:
                 net.arrived((name, "d", h - 1))
-            net.send((name, "d", h), data.at[down_slot(h - 1)], data.at[down_slot(h)], down)
+            net.send((name, "d", h), data.at[down_slot(h - 1)], data.at[down_slot(h)], down, out)
 
     def meta_hop(h):
         ring_hop("m", h, 4, 3, meta.at[:, 0])
@@ -275,7 +307,7 @@
                 for r in range(4):
                     hit = (both[r : r + 1, :] == target) & valid
                     chosen = jnp.where(hit, 1.0, chosen)
-                    weighted = jnp.where(hit, both[8 + r : 9 + r, :], weighted)
+                    weighted = jnp.where(hit, both[4 + r : 5 + r, :], weighted)
                 pick[xi, i] = chosen.astype(bf16)
                 mixed = weighted.T
                 high = mixed.astype(bf16)
@@ -297,30 +329,28 @@
             net.send(
                 (k, "y", q), chosen.at[q - 1],
                 rows.at[k, pl.ds(0, place[k][2]), pl.ds(q * toks, toks), :], ahead[q],
+                ((k, "y"), chosen), ((k, "y"), chosen),
             )
 
     def gather_rows(k):
         first, second = pl.ds(0, half), pl.ds(half, half)
-        for q in range(1, PLANE // 2):
-            net.arrived((k, "y", q))
-        net.send((k, "rA"), rows.at[k, 0, first, :], rows.at[k, 1, first, :], right)
-        for q in range(PLANE // 2, PLANE):
-            net.arrived((k, "y", q))
-        net.send((k, "lB"), rows.at[k, 0, second, :], rows.at[k, 2, second, :], left)
-        net.send((k, "rB"), rows.at[k, 0, second, :], rows.at[k, 1, second, :], right)
-        net.send((k, "lA"), rows.at[k, 0, first, :], rows.at[k, 2, first, :], left)
+        net.all_arrived((k, "y"))
+        out = ((k, "x"), rows.at[k, pl.ds(0, 3)])
+        net.send((k, "rA"), rows.at[k, 0, first, :], rows.at[k, 1, first, :], right, out)
+        net.send((k, "lB"), rows.at[k, 0, second, :], rows.at[k, 2, second, :], left, out)
+        net.send((k, "rB"), rows.at[k, 0, second, :], rows.at[k, 1, second, :], right, out)
+        net.send((k, "lA"), rows.at[k, 0, first, :], rows.at[k, 2, first, :], left, out)
 
     def forward_rows(k):
         first, second = pl.ds(0, half), pl.ds(half, half)
         net.arrived((k, "rA"))
-        net.send((k, "fA"), rows.at[k, 1, first, :], rows.at[k, 3, first, :], right)
+        net.send((k, "fA"), rows.at[k, 1, first, :], rows.at[k, 3, first, :], right, ((k, "x"), rows.at[k, pl.ds(0, 3)]))
         net.arrived((k, "lB"))
-        net.send((k, "fB"), rows.at[k, 2, second, :], rows.at[k, 3, second, :], left)
+        net.send((k, "fB"), rows.at[k, 2, second, :], rows.at[k, 3, second, :], left, ((k, "x"), rows.at[k, pl.ds(0, 3)]))
 
     def expert_in(k, first, last):
         if k in WIDE:
-            for q in range(1, PLANE):
-                net.arrived((k, "y", q))
+            net.all_arrived((k, "y"))
         else:
             for name in ("rB", "lA", "fA", "fB"):
                 net.arrived((k, name))
@@ -351,11 +381,9 @@
     def expert_out(k, first):
         if first:
             weight_copies[2].wait()
-        for q in range(1, PLANE):
-            net.sent((k, "y", q))
+        net.all_sent((k, "y"))
         if k not in WIDE:
-            for name in ("rA", "lB", "rB", "lA", "fA", "fB"):
-                net.sent((k, name))
+            net.all_sent((k, "x"))
 
         def tile(i, _):
             xi, part = i // 2, lax.rem(i, 2)
@@ -369,21 +397,23 @@
         if k in WIDE:
             back = buf(k, "back")
             for q in (4, 5, 2, 3, 6, 7, 1):
-                net.send((k, "b", q), rows.at[k, pl.ds(0, NX), pl.ds(q * toks, toks), :], back.at[q - 1], behind[q])
+                net.send((k, "b", q), rows.at[k, pl.ds(0, NX), pl.ds(q * toks, toks), :], back.at[q - 1], behind[q], ((k, "b"), back), ((k, "b"), back))
         else:
-            net.send((k, "oA"), rows.at[k, 3, a, :], buf(k, "hop_r"), right)
-            net.send((k, "oB"), rows.at[k, 3, b, :], buf(k, "hop_l"), left)
-            net.send((k, "dB"), rows.at[k, 2, b, :], buf(k, "sum_r").at[b, :], right)
-            net.send((k, "dA"), rows.at[k, 1, a, :], buf(k, "sum_l").at[a, :], left)
+            out = ((k, "r"), rows.at[k, pl.ds(0, 3)])
+            net.send((k, "oA"), rows.at[k, 3, a, :], buf(k, "hop_r"), right, out)
+            net.send((k, "oB"), rows.at[k, 3, b, :], buf(k, "hop_l"), left, out)
+            net.send((k, "dB"), rows.at[k, 2, b, :], buf(k, "sum_r").at[b, :], right, out)
+            net.send((k, "dA"), rows.at[k, 1, a, :], buf(k, "sum_l").at[a, :], left, out)
 
     def reduce_hop(k):
         a, b = pl.ds(0, half), pl.ds(half, half)
+        out = ((k, "r"), rows.at[k, pl.ds(0, 3)])
         net.arrived((k, "oA"))
         rows[k, 2, a, :] = (rows[k, 2, a, :].astype(f32) + buf(k, "hop_r")[...].astype(f32)).astype(bf16)
-        net.send((k, "sA"), rows.at[k, 2, a, :], buf(k, "sum_r").at[a, :], right)
+        net.send((k, "sA"), rows.at[k, 2, a, :], buf(k, "sum_r").at[a, :], right, out)
         net.arrived((k, "oB"))
         rows[k, 1, b, :] = (rows[k, 1, b, :].astype(f32) + buf(k, "hop_l")[...].astype(f32)).astype(bf16)
-        net.send((k, "sB"), rows.at[k, 1, b, :], buf(k, "sum_l").at[b, :], left)
+        net.send((k, "sB"), rows.at[k, 1, b, :], buf(k, "sum_l").at[b, :], left, out)
 
     def reduce_rows(k):
         for name in ("dB", "dA", "sA", "sB"):
@@ -393,11 +423,10 @@
             rows[k, 0].astype(f32) + buf(k, "sum_r")[...].astype(f32) + buf(k, "sum_l")[...].astype(f32)
         ).astype(bf16)
         for q in (4, 5, 2, 3, 6, 7, 1):
-            net.send((k, "b", q), total.at[pl.ds(q * toks, toks), :], back.at[q - 1, 0], behind[q])
+            net.send((k, "b", q), total.at[pl.ds(q * toks, toks), :], back.at[q - 1, 0], behind[q], ((k, "b"), back), ((k, "b"), back))
 
     def combine(k):
-        for q in range(1, PLANE):
-            net.arrived((k, "b", q))
+        net.all_arrived((k, "b"))
         back, mixed = buf(k, "back"), buf(k, "mixed")
         for xi in range(place[k][2]):
             for i in range(NZ // 2):
@@ -423,7 +452,7 @@
                 net.arrived((k, way, h - 1))
                 value = value + landing[j].astype(f32)
             leaving[slot(j)] = value.astype(bf16)
-            net.send((k, way, h), leaving.at[slot(j)], landing.at[j - 1], to)
+            net.send((k, way, h), leaving.at[slot(j)], landing.at[j - 1], to, ((k, "l"), leaving.at[pl.ds(1, NZ - 1)]))
 
     def finish(k):
         mixed = buf(k, "mixed")
@@ -435,9 +464,9 @@
             leaving = buf(k, "leaving")
             leaving[0] = value.astype(bf16)
             last = buf(k, "last")
-            net.send((k, "X", 2), leaving.at[0, 2], last.at[2], right)
-            net.send((k, "X", 1), leaving.at[0, 1], last.at[1], left)
-            net.send((k, "X", 3), leaving.at[0, 3], last.at[3], far)
+            net.send((k, "X", 2), leaving.at[0, 2], last.at[2], right, ((k, "X"), leaving.at[0, pl.ds(1, 3)]))
+            net.send((k, "X", 1), leaving.at[0, 1], last.at[1], left, ((k, "X"), leaving.at[0, pl.ds(1, 3)]))
+            net.send((k, "X", 3), leaving.at[0, 3], last.at[3], far, ((k, "X"), leaving.at[0, pl.ds(1, 3)]))
         else:
             out_ref[:, cols(k)] = (mid_ref[:, cols(k)].astype(f32) + value[0]).astype(bf16)
 
@@ -462,13 +491,14 @@
             args = args + [done[step] == 0]
         done[step] += 1
         step(*args)
-    for name in net.copies:
-        net.sent(name)
+    net.finish()
     assert net.used == sems.shape[0], net.used
 
 
-def layer(queries, key_value, doc_rows, angles, gains, sink, out_gain, norm_gain, resid, meta, w_out, w_gate, w_up, w_down):
+def layer(operands, weights):
     bf16, f32 = jnp.bfloat16, jnp.float32
+    queries, resid = operands[0], operands[11]
+    w_out, w_gate, w_up, w_down = weights
     toks, model = resid.shape
     held, channels = queries.shape
     width = model // CHUNKS
@@ -499,16 +529,17 @@
             shapes["last"] = pltpu.VMEM((count, nx, toks, width), bf16)
         return shapes
 
-    per_narrow = 7 + 7 + 6 + 6 + 7 + 7
-    per_wide = 3 + 7 + 7 + 7 + 7 + 3
-    copies = 7 + 7 + (10 if WIDE else 0) + (CHUNKS - wides) * per_narrow + wides * per_wide
+    per_narrow = (1 + 7) + (1 + 1) + (1 + 6) + (1 + 6) + (1 + 1) + (1 + 7)
+    per_wide = (1 + 3) + (1 + 7) + (1 + 1) + (1 + 1) + (1 + 7) + (1 + 3)
+    semaphores = (CHUNKS - wides) * per_narrow + wides * per_wide
+    semaphores += (1 + 7) + ((1 + 3) + (1 + 7) if WIDE else 0) + 2 * 7
     any_spec = pl.BlockSpec(memory_space=pl.ANY)
     vmem_spec = pl.BlockSpec(memory_space=pltpu.VMEM)
     narrow_shapes, wide_shapes = group(CHUNKS - wides, 1), group(wides, NX)
     names_n, names_w = list(narrow_shapes), list(wide_shapes)
 
     def body(*refs):
-        fixed, rest = refs[:33], refs[33:]
+        fixed, rest = refs[:37], refs[37:]
         scr_n = dict(zip(names_n, rest[: len(names_n)]))
         rest = rest[len(names_n) :]
         scr_w = dict(zip(names_w, rest[: len(names_w)]))
@@ -519,7 +550,7 @@
     return pl.pallas_call(
         body,
         out_shape=jax.ShapeDtypeStruct((toks, model), bf16),
-        in_specs=[vmem_spec] * 10 + [any_spec] * 4,
+        in_specs=[vmem_spec] * len(operands) + [any_spec] * 4,
         out_specs=vmem_spec,
         scratch_shapes=[
             pltpu.VMEM(w_out.shape, bf16),
@@ -540,27 +571,23 @@
             *tables,
             *narrow_shapes.values(),
             *wide_shapes.values(),
-            pltpu.SemaphoreType.DMA((2 * copies,)),
+            pltpu.SemaphoreType.DMA((semaphores,)),
             pltpu.SemaphoreType.DMA((4,)),
         ],
         compiler_params=pltpu.CompilerParams(
             collective_id=0, has_side_effects=True, vmem_limit_bytes=VMEM_LIMIT
         ),
         name="layer",
-    )(queries, key_value, doc_rows, angles, gains, sink, out_gain, norm_gain, resid, meta, w_out, w_gate, w_up, w_down)
-
-
-def route_table(own_routes, weights):
+    )(*operands, *weights)
+
+
+def route_slots(own_routes):
     routes = own_routes.T
-    top, toks = routes.shape
-    ids = jnp.arange(toks, dtype=jnp.int32)
+    ids = jnp.arange(routes.shape[1], dtype=jnp.int32)
     same = routes[:, :, None, None] == routes[None, None, :, :]
     earlier = ids[None, None, None, :] < ids[None, :, None, None]
     rank = jnp.sum((same & earlier).astype(jnp.int32), axis=(2, 3))
-    slots = (routes * CAP + rank).astype(jnp.float32)
-    pad = jnp.full((8 - top, toks), -1.0, jnp.float32)
-    table = jnp.concatenate([slots, pad, weights.T, pad], axis=0)
-    return jnp.concatenate([table, table], axis=1)
+    return (routes * CAP + rank).astype(jnp.float32)
 
 
 def per_device(
@@ -590,26 +617,14 @@
     half = HEAD // 2
     freqs = rope_base ** (-jnp.arange(half, dtype=f32) / half)
     turns = positions[:, None] * jnp.tile(freqs, 2 * HEAD // half)[None, :]
-    angles = jnp.concatenate([jnp.cos(turns), jnp.sin(turns)], axis=1)
-    gains = jnp.stack([jnp.tile(q_gain, 2), jnp.tile(key_norm_gain, 2)])
     quarter = held // lax.axis_size("tp")
     own_routes = lax.dynamic_slice_in_dim(routes, tp_index * quarter, quarter, 0)
-    return layer(
-        queries,
-        jnp.concatenate([keys, values], axis=1),
-        jnp.broadcast_to(docs.astype(f32)[None, :], (8, held)),
-        angles,
-        gains,
-        sink[None, :],
-        out_gain[None, :],
-        norm_gain[None, :],
-        resid,
-        route_table(own_routes, route_weights),
-        w_out,
-        w_gate,
-        w_up,
-        w_down,
+    operands = (
+        queries, keys.T, values.T, docs[None, :], jnp.cos(turns), jnp.sin(turns), q_gain[None, :],
+        key_norm_gain[None, :], sink[None, :], out_gain[None, :], norm_gain[None, :], resid,
+        route_slots(own_routes), route_weights.T,
     )
+    return layer(operands, (w_out, w_gate, w_up, w_down))
 
 
 def solution(mesh):

time: 193 us -> 183 us (0.948)
  Pallas kernels: 181 us -> 177 us
  local copies, waits for them, and re-layouts: 6.33 us -> 2.52 us
  other arithmetic: 5.68 us -> 2.86 us
    pallas_call x1, Pallas kernels: 181 us -> 177 us  [layer(): pl.pallas_call(body, out_shape=jax.ShapeDtypeStruct((toks, model), bf16),...]
    concatenate x3 -> x0, other arithmetic: 2.87 us -> none  [the longest x1 1.43 us: route_table(): return jnp.concatenate([table, table], axis=1)]
where the time goes in v4:
time: 183 us
  Pallas kernels  177 us (97%)
  other arithmetic  2.86 us (2%)
  local copies, waits for them, and re-layouts  2.52 us (1%)
    pallas_call x1, Pallas kernels, layer(): pl.pallas_call(body, out_shape=jax.ShapeDtypeStruct((toks, model), bf16),...  177 us

profile of v4, /device:TPU:8, one launch (start us, length us, event | category | flops | bytes accessed | tf_op | source)
XLA Modules:
  0.0 182.9 jit_solution(12473536702170040770)
XLA Ops:
  0.0 0.1 mul.29
  0.1 0.8 dynamic-slice_bitcast_fusion
  0.9 0.3 convert_reduce_fusion
  1.1 1.3 add_convert_fusion.refs_12_
  2.5 1.2 multiply_sine_fusion
  3.7 177.5 %layer.1 = bf16[64,2048]{1,0:T(8,128)(2,1)} custom-call(bf16[256,256]{1,0:T(8,128)(2,1)} %refs_0_.1, bf16[64,256]{1,0:T(8,128)(2,1)} %bitcast.13, bf16[64,256]{1,0:T(8,128)(2,1)} %bitcast.14, s32[1,256]{1,0:T(1,128)} %bitcast.18, f32[256,128]{1,0:T(8,128)} %get-tuple-element.6.refs_4_, f32[256,128]{1,0:T(8,128)} %get-tuple-element.5.refs_5_, ...), custom_call_target="tpu_custom_call" | custom-call | tf_op jit(solution)/shard_map/layer/pallas_call | solution.py:550
  181.2 1.7 copy.18
  (4 shorter events, 0.0 us)

commit v5 on v4

--- a/solution.py
+++ b/solution.py
@@ -17,19 +17,19 @@
 WIDE = (6, 7)
 VMEM_LIMIT = 67_043_328
 ORDER = (
-    (0,), (1, 1), (5, 1, 1), (5, 0, 1), (4, 7), (1, 2), (4, 6), (5, 1, 2), (5, 3, 1), (1, 3), (5, 1, 3), (5, 0, 2),
-    (1, 4), (5, 1, 4), (5, 4, 1), (2, 1), (5, 0, 3), (3, 0), (5, 2, 1), (6, 1), (5, 4, 2), (5, 0, 4), (5, 5, 1),
-    (5, 3, 2), (5, 2, 2), (5, 4, 3), (7, 1), (5, 7, 1), (6, 0), (5, 4, 4), (8, 1), (5, 3, 3), (2, 2), (5, 3, 4),
-    (5, 5, 2), (7, 0), (5, 7, 2), (5, 2, 3), (6, 4), (2, 3), (6, 3), (8, 0), (5, 5, 3), (5, 2, 4), (7, 4),
-    (5, 7, 3), (5, 5, 4), (6, 2), (2, 4), (7, 3), (5, 6, 1), (5, 7, 4), (6, 5), (5, 6, 2), (8, 4), (7, 2), (3, 1),
-    (8, 3), (6, 7), (5, 6, 3), (9, 0), (8, 2), (5, 6, 4), (9, 4), (9, 1), (6, 6), (7, 5), (9, 2), (8, 5), (9, 7),
-    (9, 3), (9, 5), (9, 6), (10, 6), (10, 7), (10, 0), (10, 1), (11, 1), (11, 0), (10, 2), (10, 3), (13, 6),
-    (14, 6, 1), (12, 0), (14, 6, 2), (13, 7), (14, 7, 1), (12, 1), (13, 0), (14, 0, 1), (14, 7, 2), (11, 3),
-    (11, 2), (13, 1), (10, 4), (14, 6, 3), (12, 3), (14, 1, 1), (14, 7, 3), (12, 2), (11, 4), (14, 1, 2),
-    (14, 0, 2), (14, 6, 4), (10, 5), (14, 7, 4), (13, 2), (14, 2, 1), (12, 4), (13, 3), (14, 3, 1), (14, 1, 3),
-    (11, 5), (14, 0, 3), (14, 2, 2), (15, 6), (13, 4), (14, 4, 1), (14, 1, 4), (12, 5), (14, 3, 2), (14, 0, 4),
-    (15, 7), (14, 4, 2), (14, 2, 3), (13, 5), (14, 5, 1), (16, 6), (14, 4, 3), (14, 5, 2), (14, 3, 3), (14, 5, 3),
-    (14, 4, 4), (14, 2, 4), (15, 1), (15, 0), (14, 3, 4), (14, 5, 4), (15, 4), (15, 3), (16, 7), (15, 2), (15, 5),
+    (2, 0, 1), (2, 1, 1), (2, 0, 2), (2, 5, 1), (1, 7), (2, 1, 2), (2, 0, 3), (2, 2, 1), (2, 0, 4), (2, 1, 3),
+    (1, 6), (2, 2, 2), (2, 5, 2), (0, 0), (3, 0), (2, 1, 4), (2, 4, 1), (2, 2, 3), (2, 5, 3), (3, 1), (2, 3, 1),
+    (2, 2, 4), (2, 4, 2), (2, 6, 1), (4, 0), (3, 2), (2, 4, 3), (2, 5, 4), (2, 3, 2), (4, 1), (2, 6, 2), (5, 0),
+    (3, 5), (2, 4, 4), (2, 3, 3), (2, 6, 3), (2, 3, 4), (5, 1), (2, 7, 1), (3, 4), (4, 2), (2, 6, 4), (3, 3),
+    (4, 4), (2, 7, 2), (5, 2), (0, 1), (3, 6), (2, 7, 3), (6, 0, 1), (4, 3), (2, 7, 4), (3, 7), (5, 3), (5, 4),
+    (4, 5), (6, 2, 3), (6, 4), (5, 5), (6, 6, 7), (6, 5), (7, 6), (7, 7), (7, 0), (8, 0), (7, 1), (10, 6), (8, 1),
+    (7, 2), (11, 6, 1), (7, 3), (9, 0), (10, 7), (11, 7, 1), (9, 1), (11, 6, 2), (8, 2), (10, 0), (11, 7, 2),
+    (11, 0, 1), (8, 3), (10, 1), (11, 6, 3), (11, 1, 1), (7, 4), (11, 0, 2), (9, 2), (11, 1, 2), (9, 3), (8, 4),
+    (11, 7, 3), (7, 5), (10, 2), (11, 2, 1), (11, 6, 4), (11, 7, 4), (11, 2, 2), (11, 0, 3), (11, 1, 3), (9, 4),
+    (10, 3), (11, 3, 1), (8, 5), (11, 0, 4), (10, 4), (11, 4, 1), (9, 5), (11, 3, 2), (11, 1, 4), (11, 2, 3),
+    (11, 4, 2), (12, 7), (11, 3, 3), (12, 0), (10, 5), (11, 5, 1), (11, 3, 4), (12, 6), (13, 7), (11, 5, 2),
+    (11, 4, 3), (12, 1), (11, 5, 3), (11, 2, 4), (13, 6), (12, 3), (11, 4, 4), (11, 5, 4), (12, 2), (12, 4),
+    (12, 5),
 )
 
 
@@ -171,17 +171,268 @@
         pl.semaphore_signal(barrier, inc=1, device_id=peer, device_id_type=MESH)
     pl.semaphore_wait(barrier, len(peers))
 
+    meta_width = NX if WIDE else 1
+
+    def up_hops(k):
+        return 4 if k % 2 == 0 else 3
+
+    def up_slot(h):
+        return h
+
+    def down_slot(h):
+        return 4 if h == 4 else (0 if h == 0 else 4 + h)
+
+    def wide_first(k):
+        spread = buf(k, "spread")
+        src = spread.at[0, 0]
+        out = ((k, "w"), spread.at[0, pl.ds(1, 3)])
+        net.send((k, "w", 1), src, spread.at[0, 1], right, out)
+        net.send((k, "w", 2), src, spread.at[0, 2], left, out)
+        net.send((k, "w", 3), src, spread.at[0, 3], far, out)
+
+    def meta_first():
+        if WIDE:
+            net.send(("mw", 1), meta.at[0, 0], meta.at[0, 1], right, ("mw", meta.at[0, pl.ds(1, 3)]))
+            net.send(("mw", 2), meta.at[0, 0], meta.at[0, 2], left, ("mw", meta.at[0, pl.ds(1, 3)]))
+            net.send(("mw", 3), meta.at[0, 0], meta.at[0, 3], far, ("mw", meta.at[0, pl.ds(1, 3)]))
+
+    def ring_hop(name, h, last_up, last_down, data):
+        out = ((name, "z"), data.at[pl.ds(1, NZ - 1)])
+        if h <= last_up:
+            if h > 1:
+                net.arrived((name, "u", h - 1))
+            net.send((name, "u", h), data.at[up_slot(h - 1)], data.at[up_slot(h)], up, out)
+        if h <= last_down:
+            if h > 1:
+                net.arrived((name, "d", h - 1))
+            net.send((name, "d", h), data.at[down_slot(h - 1)], data.at[down_slot(h)], down, out)
+
+    def meta_hop(h):
+        ring_hop("m", h, 4, 3, meta.at[:, 0])
+
+    def meta_wide_hop(h):
+        if h == 1:
+            for i in (1, 2, 3):
+                net.arrived(("mw", i))
+        ring_hop("mz", h, 4, 3, meta.at[:, pl.ds(1, NX - 1)])
+
+    def token_hop(k, h):
+        if h == 1 and k in WIDE:
+            for i in (1, 2, 3):
+                net.arrived((k, "w", i))
+        ring_hop(k, h, up_hops(k), 7 - up_hops(k), buf(k, "spread"))
+
+    def tables(others):
+        indices = range(1, NX) if others else (0,)
+        if not others:
+            meta_wide_hop(4)
+        net.arrived(("mz" if others else "m", "u", 4))
+        net.arrived(("mz" if others else "m", "d", 3))
+        shape = (2 * toks, 2 * toks)
+        row = lax.broadcasted_iota(jnp.int32, shape, 0)
+        lane = lax.broadcasted_iota(jnp.int32, shape, 1)
+        expert = z * PLANE + lax.rem(p + row // 16, PLANE)
+        target = (expert * CAP + lax.rem(row, CAP)).astype(f32)
+        second = lane >= toks
+        valid = (lax.rem(row // CAP, 2) == 1) == second
+        low = lax.broadcasted_iota(jnp.int32, (16, 2 * toks), 1) < toks
+        for xi in indices:
+            for i in range(NZ // 2):
+                both = jnp.where(low, meta[2 * i, xi], meta[2 * i + 1, xi])
+                chosen = jnp.zeros(shape, f32)
+                weighted = jnp.zeros(shape, f32)
+                for r in range(4):
+                    hit = (both[r : r + 1, :] == target) & valid
+                    chosen = jnp.where(hit, 1.0, chosen)
+                    weighted = jnp.where(hit, both[4 + r : 5 + r, :], weighted)
+                pick[xi, i] = chosen.astype(bf16)
+                mixed = weighted.T
+                high = mixed.astype(bf16)
+                mix_hi[xi, i] = high
+                mix_lo[xi, i] = (mixed - high.astype(f32)).astype(bf16)
+
+    def select(k):
+        net.arrived((k, "u", up_hops(k)))
+        net.arrived((k, "d", 7 - up_hops(k)))
+        spread, chosen = buf(k, "spread"), buf(k, "chosen")
+        for xi in range(place[k][2]):
+            for i in range(NZ // 2):
+                pair = jnp.concatenate([spread[2 * i, xi], spread[2 * i + 1, xi]], axis=0)
+                got = jnp.dot(pick[xi, i], pair, preferred_element_type=f32).astype(bf16)
+                rows[k, xi, 16 * i : 16 * i + 16, :] = got[0:16]
+                for q in range(1, PLANE):
+                    chosen[q - 1, xi, 16 * i : 16 * i + 16, :] = got[16 * q : 16 * q + 16]
+        for q in (4, 5, 2, 3, 6, 7, 1):
+            net.send(
+                (k, "y", q), chosen.at[q - 1],
+                rows.at[k, pl.ds(0, place[k][2]), pl.ds(q * toks, toks), :], ahead[q],
+                ((k, "y"), chosen), ((k, "y"), chosen),
+            )
+
+    def gather_rows(k):
+        first, second = pl.ds(0, half), pl.ds(half, half)
+        net.all_arrived((k, "y"))
+        out = ((k, "x"), rows.at[k, pl.ds(0, 3)])
+        net.send((k, "rA"), rows.at[k, 0, first, :], rows.at[k, 1, first, :], right, out)
+        net.send((k, "lB"), rows.at[k, 0, second, :], rows.at[k, 2, second, :], left, out)
+        net.send((k, "rB"), rows.at[k, 0, second, :], rows.at[k, 1, second, :], right, out)
+        net.send((k, "lA"), rows.at[k, 0, first, :], rows.at[k, 2, first, :], left, out)
+
+    def forward_rows(k):
+        first, second = pl.ds(0, half), pl.ds(half, half)
+        net.arrived((k, "rA"))
+        net.send((k, "fA"), rows.at[k, 1, first, :], rows.at[k, 3, first, :], right, ((k, "x"), rows.at[k, pl.ds(0, 3)]))
+        net.arrived((k, "lB"))
+        net.send((k, "fB"), rows.at[k, 2, second, :], rows.at[k, 3, second, :], left, ((k, "x"), rows.at[k, pl.ds(0, 3)]))
+
+    def expert_in(chunks, first, last):
+        for k in chunks:
+            if k in WIDE:
+                net.all_arrived((k, "y"))
+            else:
+                for name in ("rB", "lA", "fA", "fB"):
+                    net.arrived((k, name))
+        if first:
+            weight_copies[0].wait()
+            weight_copies[1].wait()
+
+        def tile(i, _):
+            xi, part = i // 2, lax.rem(i, 2)
+            at = pl.ds(pl.multiple_of(i * half, half), half)
+            g, u = 0.0, 0.0
+            for k in chunks:
+                a = rows[k, xi, pl.ds(pl.multiple_of(part * half, half), half), :]
+                g = g + jnp.dot(a, wg[cols(k), :], preferred_element_type=f32)
+                u = u + jnp.dot(a, wu[cols(k), :], preferred_element_type=f32)
+            if not first:
+                g = g + gate_acc[at, :]
+                u = u + up_acc[at, :]
+            if last:
+                c = jnp.minimum(g, swiglu_limit)
+                u = jnp.clip(u, -swiglu_limit, swiglu_limit)
+                hidden[at, :] = ((u + 1.0) * c * jax.nn.sigmoid(swiglu_alpha * c)).astype(bf16)
+            else:
+                gate_acc[at, :] = g
+                up_acc[at, :] = u
+            return 0
+
+        lax.fori_loop(0, 2 * NX, tile, 0)
+
+    def expert_out(k, first):
+        if first:
+            weight_copies[2].wait()
+        net.all_sent((k, "y"))
+        if k not in WIDE:
+            net.all_sent((k, "x"))
+
+        def tile(i, _):
+            xi, part = i // 2, lax.rem(i, 2)
+            at = pl.ds(pl.multiple_of(i * half, half), half)
+            made = jnp.dot(hidden[at, :], wd[:, cols(k)], preferred_element_type=f32)
+            rows[k, xi, pl.ds(pl.multiple_of(part * half, half), half), :] = made.astype(bf16)
+            return 0
+
+        lax.fori_loop(0, 2 * NX, tile, 0)
+        a, b = pl.ds(0, half), pl.ds(half, half)
+        if k in WIDE:
+            back = buf(k, "back")
+            for q in (4, 5, 2, 3, 6, 7, 1):
+                net.send((k, "b", q), rows.at[k, pl.ds(0, NX), pl.ds(q * toks, toks), :], back.at[q - 1], behind[q], ((k, "b"), back), ((k, "b"), back))
+        else:
+            out = ((k, "r"), rows.at[k, pl.ds(0, 3)])
+            net.send((k, "oA"), rows.at[k, 3, a, :], buf(k, "hop_r"), right, out)
+            net.send((k, "oB"), rows.at[k, 3, b, :], buf(k, "hop_l"), left, out)
+            net.send((k, "dB"), rows.at[k, 2, b, :], buf(k, "sum_r").at[b, :], right, out)
+            net.send((k, "dA"), rows.at[k, 1, a, :], buf(k, "sum_l").at[a, :], left, out)
+
+    def reduce_hop(k):
+        a, b = pl.ds(0, half), pl.ds(half, half)
+        out = ((k, "r"), rows.at[k, pl.ds(0, 3)])
+        net.arrived((k, "oA"))
+        rows[k, 2, a, :] = (rows[k, 2, a, :].astype(f32) + buf(k, "hop_r")[...].astype(f32)).astype(bf16)
+        net.send((k, "sA"), rows.at[k, 2, a, :], buf(k, "sum_r").at[a, :], right, out)
+        net.arrived((k, "oB"))
+        rows[k, 1, b, :] = (rows[k, 1, b, :].astype(f32) + buf(k, "hop_l")[...].astype(f32)).astype(bf16)
+        net.send((k, "sB"), rows.at[k, 1, b, :], buf(k, "sum_l").at[b, :], left, out)
+
+    def reduce_rows(k):
+        for name in ("dB", "dA", "sA", "sB"):
+            net.arrived((k, name))
+        back, total = buf(k, "back"), buf(k, "total")
+        total[...] = (
+            rows[k, 0].astype(f32) + buf(k, "sum_r")[...].astype(f32) + buf(k, "sum_l")[...].astype(f32)
+        ).astype(bf16)
+        for q in (4, 5, 2, 3, 6, 7, 1):
+            net.send((k, "b", q), total.at[pl.ds(q * toks, toks), :], back.at[q - 1, 0], behind[q], ((k, "b"), back), ((k, "b"), back))
+
+    def combine(k):
+        net.all_arrived((k, "b"))
+        back, mixed = buf(k, "back"), buf(k, "mixed")
+        for xi in range(place[k][2]):
+            for i in range(NZ // 2):
+                part = slice(16 * i, 16 * i + 16)
+                own = rows[k, xi, part, :] if k in WIDE else buf(k, "total")[part, :]
+                outs = jnp.concatenate([own] + [back[q - 1, xi, part, :] for q in range(1, PLANE)], axis=0)
+                got = jnp.dot(mix_hi[xi, i], outs, preferred_element_type=f32)
+                got = got + jnp.dot(mix_lo[xi, i], outs, preferred_element_type=f32)
+                mixed[2 * i, xi] = got[:toks]
+                mixed[2 * i + 1, xi] = got[toks:]
+
+    def return_hop(k, h):
+        mixed, leaving = buf(k, "mixed"), buf(k, "leaving")
+        for way, hops, slot, landing, to in (
+            ("D", up_hops(k), up_slot, buf(k, "from_up"), down),
+            ("U", 7 - up_hops(k), down_slot, buf(k, "from_down"), up),
+        ):
+            j = hops - h + 1
+            if j < 1:
+                continue
+            value = mixed[slot(j)]
+            if h > 1:
+                net.arrived((k, way, h - 1))
+                value = value + landing[j].astype(f32)
+            leaving[slot(j)] = value.astype(bf16)
+            net.send((k, way, h), leaving.at[slot(j)], landing.at[j - 1], to, ((k, "l"), leaving.at[pl.ds(1, NZ - 1)]))
+
+    def finish(k):
+        mixed = buf(k, "mixed")
+        net.arrived((k, "D", up_hops(k)))
+        net.arrived((k, "U", 7 - up_hops(k)))
+        value = mixed[0] + buf(k, "from_up")[0].astype(f32) + buf(k, "from_down")[0].astype(f32)
+        if k in WIDE:
+            mixed[0] = value
+            leaving = buf(k, "leaving")
+            leaving[0] = value.astype(bf16)
+            last = buf(k, "last")
+            net.send((k, "X", 2), leaving.at[0, 2], last.at[2], right, ((k, "X"), leaving.at[0, pl.ds(1, 3)]))
+            net.send((k, "X", 1), leaving.at[0, 1], last.at[1], left, ((k, "X"), leaving.at[0, pl.ds(1, 3)]))
+            net.send((k, "X", 3), leaving.at[0, 3], last.at[3], far, ((k, "X"), leaving.at[0, pl.ds(1, 3)]))
+        else:
+            out_ref[:, cols(k)] = (mid_ref[:, cols(k)].astype(f32) + value[0]).astype(bf16)
+
+    def finish_wide(k):
+        mixed, last = buf(k, "mixed"), buf(k, "last")
+        value = mixed[0, 0]
+        for i in (1, 2, 3):
+            net.arrived((k, "X", i))
+            value = value + last[i].astype(f32)
+        out_ref[:, cols(k)] = (mid_ref[:, cols(k)].astype(f32) + value).astype(bf16)
+
     low_rows, high_rows = pl.ds(0, WINDOW), pl.ds(held + WINDOW, WINDOW)
     net.send("kv+", kv_span.at[pl.ds(held, WINDOW), :], kv_span.at[low_rows, :], after)
     net.send("kv-", kv_span.at[pl.ds(WINDOW, WINDOW), :], kv_span.at[high_rows, :], before)
     net.send("doc+", doc_span.at[:, pl.ds(held, WINDOW)], doc_span.at[:, low_rows], after)
     net.send("doc-", doc_span.at[:, pl.ds(WINDOW, WINDOW)], doc_span.at[:, high_rows], before)
+    meta_first()
+    meta_hop(1)
     pairs = q_ref.shape[1] // lanes
     for i in range(pairs):
         part = slice(i * lanes, (i + 1) * lanes)
         q_rot[:, part] = normed_rotated(q_ref[:, part].astype(f32), q_gain).astype(bf16)
     for name in ("kv+", "kv-", "doc+", "doc-"):
         net.arrived(name)
+    meta_hop(2)
+    meta_wide_hop(1)
     both = kv_span[...].astype(f32)
     swapped = pltpu.roll(both, HEAD, axis=1)
     on_key = lax.broadcasted_iota(jnp.int32, both.shape, 1) < HEAD
@@ -209,6 +460,8 @@
         other = pl.multiple_of(lax.rem(x + d, NX) * toks, toks)
         net.send(("att", d), att.at[pl.ds(other, toks), :], by_token.at[x], peer)
     by_token[x] = att[pl.ds(pl.multiple_of(x * toks, toks), toks), :]
+    meta_hop(3)
+    meta_wide_hop(2)
     project_copy.wait()
     for d in (1, 2, 3):
         net.arrived(("att", d))
@@ -235,261 +488,22 @@
     for k in range(CHUNKS):
         value = mid_ref[:, cols(k)].astype(f32) * inverse * norm_gain_ref[0:1, cols(k)]
         buf(k, "spread")[0, 0] = value.astype(bf16)
-
-    meta_width = NX if WIDE else 1
-
-    def up_hops(k):
-        return 4 if k % 2 == 0 else 3
-
-    def up_slot(h):
-        return h
-
-    def down_slot(h):
-        return 4 if h == 4 else (0 if h == 0 else 4 + h)
-
-    def wide_first(k):
-        spread = buf(k, "spread")
-        src = spread.at[0, 0]
-        out = ((k, "w"), spread.at[0, pl.ds(1, 3)])
-        net.send((k, "w", 1), src, spread.at[0, 1], right, out)
-        net.send((k, "w", 2), src, spread.at[0, 2], left, out)
-        net.send((k, "w", 3), src, spread.at[0, 3], far, out)
-
-    def meta_first():
-        if WIDE:
-            net.send(("mw", 1), meta.at[0, 0], meta.at[0, 1], right, ("mw", meta.at[0, pl.ds(1, 3)]))
-            net.send(("mw", 2), meta.at[0, 0], meta.at[0, 2], left, ("mw", meta.at[0, pl.ds(1, 3)]))
-            net.send(("mw", 3), meta.at[0, 0], meta.at[0, 3], far, ("mw", meta.at[0, pl.ds(1, 3)]))
-
-    def ring_hop(name, h, last_up, last_down, data):
-        out = ((name, "z"), data.at[pl.ds(1, NZ - 1)])
-        if h <= last_up:
-            if h > 1:
-                net.arrived((name, "u", h - 1))
-            net.send((name, "u", h), data.at[up_slot(h - 1)], data.at[up_slot(h)], up, out)
-        if h <= last_down:
-            if h > 1:
-                net.arrived((name, "d", h - 1))
-            net.send((name, "d", h), data.at[down_slot(h - 1)], data.at[down_slot(h)], down, out)
-
-    def meta_hop(h):
-        ring_hop("m", h, 4, 3, meta.at[:, 0])
-
-    def meta_wide_hop(h):
-        if h == 1:
-            for i in (1, 2, 3):
-                net.arrived(("mw", i))
-        ring_hop("mz", h, 4, 3, meta.at[:, pl.ds(1, NX - 1)])
-
-    def token_hop(k, h):
-        if h == 1 and k in WIDE:
-            for i in (1, 2, 3):
-                net.arrived((k, "w", i))
-        ring_hop(k, h, up_hops(k), 7 - up_hops(k), buf(k, "spread"))
-
-    def tables(others):
-        indices = range(1, NX) if others else (0,)
-        net.arrived(("mz" if others else "m", "u", 4))
-        net.arrived(("mz" if others else "m", "d", 3))
-        shape = (2 * toks, 2 * toks)
-        row = lax.broadcasted_iota(jnp.int32, shape, 0)
-        lane = lax.broadcasted_iota(jnp.int32, shape, 1)
-        expert = z * PLANE + lax.rem(p + row // 16, PLANE)
-        target = (expert * CAP + lax.rem(row, CAP)).astype(f32)
-        second = lane >= toks
-        valid = (lax.rem(row // CAP, 2) == 1) == second
-        low = lax.broadcasted_iota(jnp.int32, (16, 2 * toks), 1) < toks
-        for xi in indices:
-            for i in range(NZ // 2):
-                both = jnp.where(low, meta[2 * i, xi], meta[2 * i + 1, xi])
-                chosen = jnp.zeros(shape, f32)
-                weighted = jnp.zeros(shape, f32)
-                for r in range(4):
-                    hit = (both[r : r + 1, :] == target) & valid
-                    chosen = jnp.where(hit, 1.0, chosen)
-                    weighted = jnp.where(hit, both[4 + r : 5 + r, :], weighted)
-                pick[xi, i] = chosen.astype(bf16)
-                mixed = weighted.T
-                high = mixed.astype(bf16)
-                mix_hi[xi, i] = high
-                mix_lo[xi, i] = (mixed - high.astype(f32)).astype(bf16)
-
-    def select(k):
-        net.arrived((k, "u", up_hops(k)))
-        net.arrived((k, "d", 7 - up_hops(k)))
-        spread, chosen = buf(k, "spread"), buf(k, "chosen")
-        for xi in range(place[k][2]):
-            for i in range(NZ // 2):
-                pair = jnp.concatenate([spread[2 * i, xi], spread[2 * i + 1, xi]], axis=0)
-                got = jnp.dot(pick[xi, i], pair, preferred_element_type=f32).astype(bf16)
-                rows[k, xi, 16 * i : 16 * i + 16, :] = got[0:16]
-                for q in range(1, PLANE):
-                    chosen[q - 1, xi, 16 * i : 16 * i + 16, :] = got[16 * q : 16 * q + 16]
-        for q in (4, 5, 2, 3, 6, 7, 1):
-            net.send(
-                (k, "y", q), chosen.at[q - 1],
-                rows.at[k, pl.ds(0, place[k][2]), pl.ds(q * toks, toks), :], ahead[q],
-                ((k, "y"), chosen), ((k, "y"), chosen),
-            )
-
-    def gather_rows(k):
-        first, second = pl.ds(0, half), pl.ds(half, half)
-        net.all_arrived((k, "y"))
-        out = ((k, "x"), rows.at[k, pl.ds(0, 3)])
-        net.send((k, "rA"), rows.at[k, 0, first, :], rows.at[k, 1, first, :], right, out)
-        net.send((k, "lB"), rows.at[k, 0, second, :], rows.at[k, 2, second, :], left, out)
-        net.send((k, "rB"), rows.at[k, 0, second, :], rows.at[k, 1, second, :], right, out)
-        net.send((k, "lA"), rows.at[k, 0, first, :], rows.at[k, 2, first, :], left, out)
-
-    def forward_rows(k):
-        first, second = pl.ds(0, half), pl.ds(half, half)
-        net.arrived((k, "rA"))
-        net.send((k, "fA"), rows.at[k, 1, first, :], rows.at[k, 3, first, :], right, ((k, "x"), rows.at[k, pl.ds(0, 3)]))
-        net.arrived((k, "lB"))
-        net.send((k, "fB"), rows.at[k, 2, second, :], rows.at[k, 3, second, :], left, ((k, "x"), rows.at[k, pl.ds(0, 3)]))
-
-    def expert_in(k, first, last):
-        if k in WIDE:
-            net.all_arrived((k, "y"))
-        else:
-            for name in ("rB", "lA", "fA", "fB"):
-                net.arrived((k, name))
-        if first:
-            weight_copies[0].wait()
-            weight_copies[1].wait()
-
-        def tile(i, _):
-            xi, part = i // 2, lax.rem(i, 2)
-            a = rows[k, xi, pl.ds(pl.multiple_of(part * half, half), half), :]
-            at = pl.ds(pl.multiple_of(i * half, half), half)
-            g = jnp.dot(a, wg[cols(k), :], preferred_element_type=f32)
-            u = jnp.dot(a, wu[cols(k), :], preferred_element_type=f32)
-            if not first:
-                g = g + gate_acc[at, :]
-                u = u + up_acc[at, :]
-            if last:
-                c = jnp.minimum(g, swiglu_limit)
-                u = jnp.clip(u, -swiglu_limit, swiglu_limit)
-                hidden[at, :] = ((u + 1.0) * c * jax.nn.sigmoid(swiglu_alpha * c)).astype(bf16)
-            else:
-                gate_acc[at, :] = g
-                up_acc[at, :] = u
-            return 0
-
-        lax.fori_loop(0, 2 * NX, tile, 0)
-
-    def expert_out(k, first):
-        if first:
-            weight_copies[2].wait()
-        net.all_sent((k, "y"))
-        if k not in WIDE:
-            net.all_sent((k, "x"))
-
-        def tile(i, _):
-            xi, part = i // 2, lax.rem(i, 2)
-            at = pl.ds(pl.multiple_of(i * half, half), half)
-            made = jnp.dot(hidden[at, :], wd[:, cols(k)], preferred_element_type=f32)
-            rows[k, xi, pl.ds(pl.multiple_of(part * half, half), half), :] = made.astype(bf16)
-            return 0
-
-        lax.fori_loop(0, 2 * NX, tile, 0)
-        a, b = pl.ds(0, half), pl.ds(half, half)
-        if k in WIDE:
-            back = buf(k, "back")
-            for q in (4, 5, 2, 3, 6, 7, 1):
-                net.send((k, "b", q), rows.at[k, pl.ds(0, NX), pl.ds(q * toks, toks), :], back.at[q - 1], behind[q], ((k, "b"), back), ((k, "b"), back))
-        else:
-            out = ((k, "r"), rows.at[k, pl.ds(0, 3)])
-            net.send((k, "oA"), rows.at[k, 3, a, :], buf(k, "hop_r"), right, out)
-            net.send((k, "oB"), rows.at[k, 3, b, :], buf(k, "hop_l"), left, out)
-            net.send((k, "dB"), rows.at[k, 2, b, :], buf(k, "sum_r").at[b, :], right, out)
-            net.send((k, "dA"), rows.at[k, 1, a, :], buf(k, "sum_l").at[a, :], left, out)
-
-    def reduce_hop(k):
-        a, b = pl.ds(0, half), pl.ds(half, half)
-        out = ((k, "r"), rows.at[k, pl.ds(0, 3)])
-        net.arrived((k, "oA"))
-        rows[k, 2, a, :] = (rows[k, 2, a, :].astype(f32) + buf(k, "hop_r")[...].astype(f32)).astype(bf16)
-        net.send((k, "sA"), rows.at[k, 2, a, :], buf(k, "sum_r").at[a, :], right, out)
-        net.arrived((k, "oB"))
-        rows[k, 1, b, :] = (rows[k, 1, b, :].astype(f32) + buf(k, "hop_l")[...].astype(f32)).astype(bf16)
-        net.send((k, "sB"), rows.at[k, 1, b, :], buf(k, "sum_l").at[b, :], left, out)
-
-    def reduce_rows(k):
-        for name in ("dB", "dA", "sA", "sB"):
-            net.arrived((k, name))
-        back, total = buf(k, "back"), buf(k, "total")
-        total[...] = (
-            rows[k, 0].astype(f32) + buf(k, "sum_r")[...].astype(f32) + buf(k, "sum_l")[...].astype(f32)
-        ).astype(bf16)
-        for q in (4, 5, 2, 3, 6, 7, 1):
-            net.send((k, "b", q), total.at[pl.ds(q * toks, toks), :], back.at[q - 1, 0], behind[q], ((k, "b"), back), ((k, "b"), back))
-
-    def combine(k):
-        net.all_arrived((k, "b"))
-        back, mixed = buf(k, "back"), buf(k, "mixed")
-        for xi in range(place[k][2]):
-            for i in range(NZ // 2):
-                part = slice(16 * i, 16 * i + 16)
-                own = rows[k, xi, part, :] if k in WIDE else buf(k, "total")[part, :]
-                outs = jnp.concatenate([own] + [back[q - 1, xi, part, :] for q in range(1, PLANE)], axis=0)
-                got = jnp.dot(mix_hi[xi, i], outs, preferred_element_type=f32)
-                got = got + jnp.dot(mix_lo[xi, i], outs, preferred_element_type=f32)
-                mixed[2 * i, xi] = got[:toks]
-                mixed[2 * i + 1, xi] = got[toks:]
-
-    def return_hop(k, h):
-        mixed, leaving = buf(k, "mixed"), buf(k, "leaving")
-        for way, hops, slot, landing, to in (
-            ("D", up_hops(k), up_slot, buf(k, "from_up"), down),
-            ("U", 7 - up_hops(k), down_slot, buf(k, "from_down"), up),
-        ):
-            j = hops - h + 1
-            if j < 1:
-                continue
-            value = mixed[slot(j)]
-            if h > 1:
-                net.arrived((k, way, h - 1))
-                value = value + landing[j].astype(f32)
-            leaving[slot(j)] = value.astype(bf16)
-            net.send((k, way, h), leaving.at[slot(j)], landing.at[j - 1], to, ((k, "l"), leaving.at[pl.ds(1, NZ - 1)]))
-
-    def finish(k):
-        mixed = buf(k, "mixed")
-        net.arrived((k, "D", up_hops(k)))
-        net.arrived((k, "U", 7 - up_hops(k)))
-        value = mixed[0] + buf(k, "from_up")[0].astype(f32) + buf(k, "from_down")[0].astype(f32)
-        if k in WIDE:
-            mixed[0] = value
-            leaving = buf(k, "leaving")
-            leaving[0] = value.astype(bf16)
-            last = buf(k, "last")
-            net.send((k, "X", 2), leaving.at[0, 2], last.at[2], right, ((k, "X"), leaving.at[0, pl.ds(1, 3)]))
-            net.send((k, "X", 1), leaving.at[0, 1], last.at[1], left, ((k, "X"), leaving.at[0, pl.ds(1, 3)]))
-            net.send((k, "X", 3), leaving.at[0, 3], last.at[3], far, ((k, "X"), leaving.at[0, pl.ds(1, 3)]))
-        else:
-            out_ref[:, cols(k)] = (mid_ref[:, cols(k)].astype(f32) + value[0]).astype(bf16)
-
-    def finish_wide(k):
-        mixed, last = buf(k, "mixed"), buf(k, "last")
-        value = mixed[0, 0]
-        for i in (1, 2, 3):
-            net.arrived((k, "X", i))
-            value = value + last[i].astype(f32)
-        out_ref[:, cols(k)] = (mid_ref[:, cols(k)].astype(f32) + value).astype(bf16)
+    meta_hop(4)
+    meta_wide_hop(3)
 
     steps = (
-        meta_first, meta_hop, meta_wide_hop, tables, wide_first, token_hop, select, gather_rows, forward_rows,
+        tables, wide_first, token_hop, select, gather_rows, forward_rows,
         expert_in, expert_out, reduce_hop, reduce_rows, combine, return_hop, finish, finish_wide,
     )
     done = {step: 0 for step in steps}
     for number, *args in ORDER:
         step = steps[number]
+        first = done[step] == 0
+        done[step] += len(args) if step is expert_in else 1
         if step is expert_in:
-            args = args + [done[step] == 0, done[step] == CHUNKS - 1]
+            args = [args, first, done[step] == CHUNKS]
         if step is expert_out:
-            args = args + [done[step] == 0]
-        done[step] += 1
+            args = args + [first]
         step(*args)
     net.finish()
     assert net.used == sems.shape[0], net.used

time: 183 us -> 180 us (0.984)
  Pallas kernels: 177 us -> 174 us
    pallas_call x1, Pallas kernels: 177 us -> 174 us  [layer(): pl.pallas_call(body, out_shape=jax.ShapeDtypeStruct((toks, model), bf16),...]
where the time goes in v5:
time: 180 us; the launch traced here: 179 us
  Pallas kernels  174 us (97%)
  other arithmetic  2.86 us (2%)
  local copies, waits for them, and re-layouts  2.52 us (1%)
    pallas_call x1, Pallas kernels, layer(): pl.pallas_call(body, out_shape=jax.ShapeDtypeStruct((toks, model), bf16),...  174 us

profile of v5, /device:TPU:8, one launch (start us, length us, event | category | flops | bytes accessed | tf_op | source)
XLA Modules:
  0.0 179.3 jit_solution(18411303126143014299)
XLA Ops:
  0.0 0.1 mul.29
  0.1 0.8 dynamic-slice_bitcast_fusion
  0.9 0.3 convert_reduce_fusion
  1.1 1.3 add_convert_fusion.refs_12_
  2.5 1.2 multiply_sine_fusion
  3.7 173.9 %layer.1 = bf16[64,2048]{1,0:T(8,128)(2,1)} custom-call(bf16[256,256]{1,0:T(8,128)(2,1)} %refs_0_.1, bf16[64,256]{1,0:T(8,128)(2,1)} %bitcast.13, bf16[64,256]{1,0:T(8,128)(2,1)} %bitcast.14, s32[1,256]{1,0:T(1,128)} %bitcast.18, f32[256,128]{1,0:T(8,128)} %get-tuple-element.6.refs_4_, f32[256,128]{1,0:T(8,128)} %get-tuple-element.5.refs_5_, ...), custom_call_target="tpu_custom_call" | custom-call | tf_op jit(solution)/shard_map/layer/pallas_call | solution.py:564
  177.7 1.7 copy.18
  (4 shorter events, 0.0 us)
